TPU v7x, 32 devices: a whole 2x2x4 slice. The times are simulated.
32 devices in a mesh: sp: 8 (over z, y), tp: 4 (over x, core).
Axes of the slice: x: 2, y: 2, z: 4, core: 2. Of those that a mesh axis runs over, the one named last changes fastest.
Arguments:
- block_input: bfloat16 [8192, 2048], P('sp'), may hold values from -6 to 6
- value_proj: bfloat16 [2048, 1024], P(None, 'tp'), may hold values from -0.125 to 0.125
- gate_proj: bfloat16 [2048, 1024], P(None, 'tp'), may hold values from -0.125 to 0.125
- conv_taps: float32 [31, 1024], P(None, 'tp'), may hold values from -3 to 3
- norm_gain: float32 [1024], P('tp'), may hold values from 0.1 to 1.9
- out_proj: bfloat16 [2048, 1024], P(None, 'tp'), may hold values from -0.125 to 0.125
- grad_output: bfloat16 [8192, 2048], P('sp'), may hold values from -6 to 6
Outputs:
- input_grad: bfloat16 [8192, 2048], P('sp', 'tp')
- value_grad: float32 [2048, 1024], P('sp', 'tp')
- gate_grad: float32 [2048, 1024], P('sp', 'tp')
- out_grad: float32 [2048, 1024], P('sp', 'tp')
- taps_grad: float32 [31, 1024], P(None, 'tp')
- gain_grad: float32 [1024], P('tp')
All inputs are finite; a program needn't handle non-finite values.
Results may differ from a plain program's by a relative error of at most 0.015.
Values may be sent and summed in bfloat16 or wider, within the bound.
A program may use at most 64 MiB of HBM per device.

v0:
```python
import functools

import jax
import jax.numpy as jnp
from jax import lax
from jax.experimental import pallas as pl
from jax.experimental.pallas import tpu as pltpu
from jax.sharding import PartitionSpec as P

NORM_FLOOR = 0.1
LANES = 128
ROW_BLOCK = 128
MATMUL_ROWS = 256
PAD = 32
F32 = jnp.float32
BF16 = jnp.bfloat16
MESH = pl.DeviceIdType.MESH


def dot_nt(a, b):
    return lax.dot_general(a, b, (((1,), (1,)), ((), ())), preferred_element_type=F32)


def dot_tn(a, b):
    return lax.dot_general(a, b, (((0,), (0,)), ((), ())), preferred_element_type=F32)


def kernel(cfg, bi_hbm, wv_hbm, wg_hbm, taps_ref, gain_ref, wo_hbm, go_hbm,
           ig_ref, wgrad_ref, small_ref,
           bi, wv, wg, wo, go, val, sg, slope, hist, nrm, nsl, fut, act, sl, psl, pw,
           st1, st1r, st2, st2r, gvg, gout, yvg, yout, avg, aout, arvg, arout, bvg, bout, brvg, brout,
           xs, xr, tg, tgy, tgz, tgzr,
           ld_sem, halo_sem, st_send, st_recv, pw_send, pw_recv, sl_send, sl_recv,
           x_send, x_recv, y_send, y_recv, a_send, a_recv, b_send, b_recv, ty_send, ty_recv, tz_send, tz_recv):
    nsp, ntp, ny, nz, nx, chan = cfg
    rows, width = bi.shape
    cl = wv.shape[1]
    groups = cl // LANES
    tap_count = taps_ref.shape[0]
    nb = rows // ROW_BLOCK
    vpb = ROW_BLOCK // 8
    nrc = rows // MATMUL_ROWS
    ds = width // nsp
    dt = width // ntp
    sp = lax.axis_index("sp")
    tp = lax.axis_index("tp")
    z = sp // ny
    y = sp % ny
    x = tp // 2
    core = tp % 2

    def wrap(v, n):
        return lax.rem(v, n)

    loads = {}

    def load(name, src, dst, i):
        c = pltpu.make_async_copy(src, dst, ld_sem.at[i])
        c.start()
        loads[name] = c

    load("wv", wv_hbm, wv, 0)
    load("wg", wg_hbm, wg, 1)
    for n, i in enumerate(reversed(range(nrc))):
        s = pl.ds(i * MATMUL_ROWS, MATMUL_ROWS)
        load("bi%d" % i, bi_hbm.at[s], bi.at[s], 2 + n)
    load("wo", wo_hbm, wo, 2 + nrc)
    load("go", go_hbm, go, 3 + nrc)

    barrier = pltpu.get_barrier_semaphore()
    for o in range(1, nsp):
        pl.semaphore_signal(barrier, inc=1, device_id={"sp": wrap(sp + o, nsp)}, device_id_type=MESH)
    for o in range(1, ntp):
        pl.semaphore_signal(barrier, inc=1, device_id={"tp": wrap(tp + o, ntp)}, device_id_type=MESH)

    def remote(src, dst, ssem, rsem, dev):
        return pltpu.make_async_remote_copy(
            src_ref=src, dst_ref=dst, send_sem=ssem, recv_sem=rsem, device_id=dev, device_id_type=MESH)

    def glu(i):
        r = i * MATMUL_ROWS
        a = bi[r:r + MATMUL_ROWS, :]
        v = jnp.dot(a, wv[...], preferred_element_type=F32)
        s = jax.nn.sigmoid(jnp.dot(a, wg[...], preferred_element_type=F32))
        m = (v * s).astype(BF16).astype(F32)
        for g in range(groups):
            c = slice(g * LANES, (g + 1) * LANES)
            val[g, r:r + MATMUL_ROWS, :] = v[:, c]
            sg[g, r:r + MATMUL_ROWS, :] = s[:, c]
            hist[g, PAD + r:PAD + r + MATMUL_ROWS, :] = m[:, c]

    halo = remote(hist.at[:, pl.ds(rows, PAD), :], hist.at[:, pl.ds(0, PAD), :],
                  halo_sem.at[0], halo_sem.at[1], {"sp": jnp.minimum(sp + 1, nsp - 1)})
    back = remote(fut.at[:, pl.ds(0, PAD), :], fut.at[:, pl.ds(rows, PAD), :],
                  halo_sem.at[2], halo_sem.at[3], {"sp": jnp.maximum(sp - 1, 0)})
    has_next = sp < nsp - 1
    has_prev = sp > 0

    @pl.when(jnp.logical_not(has_prev))
    def _():
        hist[:, 0:PAD, :] = jnp.zeros((groups, PAD, LANES), F32)

    @pl.when(jnp.logical_not(has_next))
    def _():
        fut[:, rows:rows + PAD, :] = jnp.zeros((groups, PAD, LANES), F32)

    loads["wv"].wait()
    loads["wg"].wait()
    partner = {"tp": 2 * x + 1 - core}
    pws = []
    for n, i in enumerate(reversed(range(nrc))):
        loads["bi%d" % i].wait()
        glu(i)
        if n == 0:
            pl.semaphore_wait(barrier, nsp + ntp - 2)

            @pl.when(has_next)
            def _():
                halo.start()

            for xx in range(nx):
                for j, w in enumerate((wv, wg)):
                    first = pl.multiple_of((2 * xx + 1 - core) * dt, dt)
                    c = remote(w.at[pl.ds(first, dt), :], pw.at[xx, j], pw_send.at[xx, j], pw_recv.at[xx, j], partner)
                    c.start()
                    pws.append(c)

    lane = lax.broadcasted_iota(jnp.int32, (8, LANES), 1)

    def pack(packed, red, b):
        for i in range(vpb):
            packed = jnp.where(lane == b * vpb + i, red[8 * i:8 * i + 8], packed)
        return packed

    def unpack(rolled):
        return jnp.concatenate([rolled[:, i:i + 1] for i in range(vpb)], axis=0)

    def roll_to(packed, b):
        return pltpu.roll(packed, lax.rem(LANES - b * vpb, LANES), 1)

    def tap(k, g):
        return taps_ref[k:k + 1, g * LANES:(g + 1) * LANES]

    def conv_block(b, carry):
        psum, psq = carry
        s = q = None
        for g in range(groups):
            acc = jnp.zeros((ROW_BLOCK, LANES), F32)
            for k in range(tap_count):
                acc = acc + tap(k, g) * hist[g, pl.ds(b * ROW_BLOCK + (PAD - k), ROW_BLOCK), :]
            nrm[g, pl.ds(pl.multiple_of(b * ROW_BLOCK, ROW_BLOCK), ROW_BLOCK), :] = acc
            s = acc if s is None else s + acc
            q = acc * acc if q is None else q + acc * acc
        return (pack(psum, jnp.sum(s, axis=1, keepdims=True), b),
                pack(psq, jnp.sum(q, axis=1, keepdims=True), b))

    zero = jnp.zeros((8, LANES), F32)
    carry = lax.fori_loop(0, nb - 1, lambda i, c: conv_block(nb - 1 - i, c), (zero, zero))

    @pl.when(has_prev)
    def _():
        halo.wait_recv()

    psum, psq = conv_block(0, carry)
    st1[0] = psum
    st1[1] = psq

    def share(which, src, dst):
        out = []
        for o in range(1, ntp):
            c = remote(src, dst.at[o - 1], st_send.at[which, o - 1], st_recv.at[which, o - 1],
                       {"tp": wrap(tp + o, ntp)})
            c.start()
            out.append(c)
        return out

    st_copies = share(0, st1, st1r)

    loads["wo"].wait()
    loads["go"].wait()
    for i in range(nrc):
        r = i * MATMUL_ROWS
        t = jnp.dot(go[r:r + MATMUL_ROWS, :], wo[...], preferred_element_type=F32)
        for g in range(groups):
            slope[g, r:r + MATMUL_ROWS, :] = t[:, g * LANES:(g + 1) * LANES]

    for c in st_copies:
        c.wait()
    tsum, tsq = st1[0], st1[1]
    for o in range(ntp - 1):
        tsum = tsum + st1r[o, 0]
        tsq = tsq + st1r[o, 1]
    center = tsum / chan
    inverse = lax.rsqrt(tsq / chan - center * center + NORM_FLOOR)

    def norm_block(b, carry):
        psum, pcross, gacc = carry
        r = pl.ds(pl.multiple_of(b * ROW_BLOCK, ROW_BLOCK), ROW_BLOCK)
        cen = unpack(roll_to(center, b))
        inv = unpack(roll_to(inverse, b))
        s = q = None
        gout_acc = []
        for g in range(groups):
            gain = gain_ref[:, g * LANES:(g + 1) * LANES]
            normed = (nrm[g, r, :] - cen) * inv
            scaled = normed * gain
            squash = jax.nn.sigmoid(scaled)
            act[r, g * LANES:(g + 1) * LANES] = (scaled * squash).astype(BF16)
            pre = slope[g, r, :] * squash * (1.0 + scaled * (1.0 - squash))
            pn = pre * normed
            tot = gacc[g]
            for i in range(vpb):
                tot = tot + pn[8 * i:8 * i + 8]
            gout_acc.append(tot)
            ns = pre * gain
            nrm[g, r, :] = normed
            nsl[g, r, :] = ns * inv
            cross = ns * normed
            s = ns if s is None else s + ns
            q = cross if q is None else q + cross
        return (pack(psum, jnp.sum(s, axis=1, keepdims=True), b),
                pack(pcross, jnp.sum(q, axis=1, keepdims=True), b), tuple(gout_acc))

    psum, pcross, gacc = lax.fori_loop(0, nb, norm_block, (zero, zero, (zero,) * groups))
    st2[0] = psum
    st2[1] = pcross
    st_copies = share(1, st2, st2r)

    per = max(1, min(256, width) // ds)
    zh = z // 2
    zl = z % 2
    nh = nz // 2

    def plane(u):
        side = zl if u % 2 else 1 - zl
        return 2 * wrap(zh + u // 2 + 1, nh) + side

    peers = [(u, r) for u in range(nz) for r in range(1, ny)]

    def y_copies(which, src, dst):
        out = {}
        for o, r in peers:
            yy = wrap(y + r, ny)
            out[o, r] = remote(src.at[plane(o) * ny + yy], dst.at[r - 1, o], y_send.at[which, r - 1, o],
                               y_recv.at[which, r - 1, o], {"sp": z * ny + yy})
        return out

    def weight_chunk(src, right, dst, chunk):
        cols = pl.ds(pl.multiple_of(chunk * per * ds, per * ds), per * ds)
        t = dot_tn(src[:, cols], right[...]).astype(BF16)
        for j in range(per):
            dst[chunk * per + j] = t[j * ds:(j + 1) * ds]

    def weight_peer_part(src, right, dst, copies):
        if per == 1:
            for o, r in peers:
                weight_chunk(src, right, dst, plane(o) * ny + wrap(y + r, ny))
                copies[o, r].start()
        else:
            for chunk in range(nsp // per):
                weight_chunk(src, right, dst, chunk)
            for o, r in peers:
                copies[o, r].start()

    def weight_own_part(src, right, dst):
        if per == 1:
            for o in range(nz):
                weight_chunk(src, right, dst, plane(o) * ny + y)

    yc_out = y_copies(0, gout, yout)
    yc_vg = y_copies(1, gvg, yvg)
    weight_peer_part(go, act, gout, yc_out)

    for c in st_copies:
        c.wait()
    tsum, tcross = st2[0], st2[1]
    for o in range(ntp - 1):
        tsum = tsum + st2r[o, 0]
        tcross = tcross + st2r[o, 1]
    tsum = tsum / chan * inverse
    tcross = tcross / chan * inverse

    def slope_block(b, c):
        r = pl.ds(pl.multiple_of(b * ROW_BLOCK, ROW_BLOCK), ROW_BLOCK)
        ss = unpack(roll_to(tsum, b))
        cs = unpack(roll_to(tcross, b))
        for g in range(groups):
            fut[g, r, :] = nsl[g, r, :] - ss - nrm[g, r, :] * cs
        return c

    slope_block(0, 0)

    @pl.when(has_prev)
    def _():
        back.start()

    lax.fori_loop(1, nb, slope_block, 0)

    def adjoint_block(b, c):
        r = pl.ds(pl.multiple_of(b * ROW_BLOCK, ROW_BLOCK), ROW_BLOCK)
        for g in range(groups):
            acc = jnp.zeros((ROW_BLOCK, LANES), F32)
            for k in range(tap_count):
                acc = acc + tap(k, g) * fut[g, pl.ds(b * ROW_BLOCK + k, ROW_BLOCK), :]
            s = sg[g, r, :]
            t = acc * s
            sl[r, g * LANES:(g + 1) * LANES] = t.astype(BF16)
            sl[r, cl + g * LANES:cl + (g + 1) * LANES] = (t * val[g, r, :] * (1.0 - s)).astype(BF16)
        return c

    def input_part(i, xx):
        r = slice(i * MATMUL_ROWS, (i + 1) * MATMUL_ROWS)
        blk = pl.ds(pl.multiple_of((2 * xx + core) * dt, dt), dt)
        t = dot_nt(sl[r, 0:cl], wv[blk, :]) + dot_nt(sl[r, cl:2 * cl], wg[blk, :])
        return t + dot_nt(psl[r, 0:cl], pw[xx, 0]) + dot_nt(psl[r, cl:2 * cl], pw[xx, 1])

    xc = []

    def input_send(i):
        slc[i].wait()
        for o in range(1, nx):
            xx = wrap(x + o, nx)
            xs[o - 1, i] = input_part(i, xx).astype(BF16)
            c = remote(xs.at[o - 1, i], xr.at[o - 1, i], x_send.at[o - 1, i], x_recv.at[o - 1, i],
                       {"tp": 2 * xx + core})
            c.start()
            xc.append(c)

    for c in pws:
        c.wait()
    bpc = MATMUL_ROWS // ROW_BLOCK
    slc = []
    for i in range(nrc):
        if i == nrc - 1:
            lax.fori_loop(i * bpc, nb - 1, adjoint_block, 0)

            @pl.when(has_next)
            def _():
                back.wait_recv()

            adjoint_block(nb - 1, 0)
        else:
            lax.fori_loop(i * bpc, (i + 1) * bpc, adjoint_block, 0)
        s = pl.ds(i * MATMUL_ROWS, MATMUL_ROWS)
        c = remote(sl.at[s], psl.at[s], sl_send.at[i], sl_recv.at[i], partner)
        c.start()
        slc.append(c)
        if i > 0:
            input_send(i - 1)

    weight_peer_part(bi, sl, gvg, yc_vg)
    input_send(nrc - 1)

    weight_own_part(go, act, gout)
    weight_own_part(bi, sl, gvg)

    def y_sum(u, gb, yb, ycs):
        t = gb[plane(u) * ny + y].astype(F32)
        for r in range(1, ny):
            ycs[u, r].wait()
            t = t + yb[r - 1, u].astype(F32)
        return t

    pair = {"sp": (2 * zh + 1 - zl) * ny + y}
    across = {}

    def a_step(which, h):
        gb, yb, ycs, buf, rbuf = ((gout, yout, yc_out, aout, arout), (gvg, yvg, yc_vg, avg, arvg))[which]
        buf[h] = y_sum(2 * h, gb, yb, ycs).astype(BF16)
        c = remote(buf.at[h], rbuf.at[h], a_send.at[which, h], a_recv.at[which, h], pair)
        c.start()
        across[which, h] = c

    def b_sum(which, h):
        gb, yb, ycs, rbuf = ((gout, yout, yc_out, arout), (gvg, yvg, yc_vg, arvg))[which]
        t = y_sum(2 * h + 1, gb, yb, ycs)
        across[which, h].wait()
        return t + rbuf[h].astype(F32)

    b_copies = {}

    def b_step(which, h):
        buf, rbuf = ((bout, brout), (bvg, brvg))[which]
        buf[h] = b_sum(which, h).astype(BF16)
        c = remote(buf.at[h], rbuf.at[h], b_send.at[which, h], b_recv.at[which, h],
                   {"sp": (2 * wrap(zh + h + 1, nh) + zl) * ny + y})
        c.start()
        b_copies[which, h] = c

    def final_sum(which):
        rbuf = (brout, brvg)[which]
        t = b_sum(which, nh - 1)
        for h in range(nh - 1):
            b_copies[which, h].wait()
            t = t + rbuf[h].astype(F32)
        return t

    for h in range(nh):
        a_step(0, h)

    step = 4
    for g in range(groups):
        def tap_block(b, accs, g=g):
            r = b * 8 * step
            f = fut[g, pl.ds(pl.multiple_of(r, 8 * step), 8 * step), :]
            out = []
            for k in range(tap_count):
                p = f * hist[g, pl.ds(r + (PAD - k), 8 * step), :]
                t = accs[k]
                for i in range(step):
                    t = t + p[8 * i:8 * i + 8]
                out.append(t)
            return tuple(out)

        accs = lax.fori_loop(0, rows // (8 * step), tap_block, (zero,) * tap_count)
        for k in range(tap_count):
            tg[k:k + 1, g * LANES:(g + 1) * LANES] = jnp.sum(accs[k], axis=0, keepdims=True)
        tg[tap_count:tap_count + 1, g * LANES:(g + 1) * LANES] = jnp.sum(gacc[g], axis=0, keepdims=True)

    tzc = []
    for o in range(1, nz):
        c = remote(tg, tgzr.at[o - 1], tz_send.at[o - 1], tz_recv.at[o - 1], {"sp": wrap(z + o, nz) * ny + y})
        c.start()
        tzc.append(c)

    for h in range(nh - 1):
        b_step(0, h)
    a_step(1, 0)
    t = tg[...]
    for o in range(1, nz):
        tzc[o - 1].wait()
        t = t + tgzr[o - 1]
    tgz[...] = t
    tyc = []
    for r in range(1, ny):
        c = remote(tgz, tgy.at[r - 1], ty_send.at[r - 1], ty_recv.at[r - 1], {"sp": z * ny + wrap(y + r, ny)})
        c.start()
        tyc.append(c)
    for h in range(nh - 1):
        b_step(1, h)
        a_step(1, h + 1)

    wgrad_ref[2] = final_sum(0)

    for i in range(nrc):
        t = input_part(i, x)
        for o in range(1, nx):
            xc[i * (nx - 1) + o - 1].wait()
            t = t + xr[o - 1, i].astype(F32)
        ig_ref[i * MATMUL_ROWS:(i + 1) * MATMUL_ROWS, :] = t.astype(BF16)


    own = final_sum(1)
    wgrad_ref[0] = own[:, 0:cl]
    wgrad_ref[1] = own[:, cl:2 * cl]

    t = tgz[...]
    for r in range(1, ny):
        tyc[r - 1].wait()
        t = t + tgy[r - 1]
    small_ref[...] = t

    @pl.when(has_next)
    def _():
        halo.wait_send()

    @pl.when(has_prev)
    def _():
        back.wait_send()


def hand_out(ig_in, wgrad_in, small_in, ig_ref, vgrad_ref, ggrad_ref, ograd_ref, tgrad_ref, gaingrad_ref,
             ig, wgrad, small, taps, gain, in_sem, out_sem):
    tap_count = tgrad_ref.shape[0]
    parts = ig.shape[0] // MATMUL_ROWS
    moves = [(small_in, small, ((taps, tgrad_ref), (gain, gaingrad_ref)))]
    for i in range(parts):
        s = pl.ds(i * MATMUL_ROWS, MATMUL_ROWS)
        moves.append((ig_in.at[s], ig.at[s], ((ig.at[s], ig_ref.at[s]),)))
    for i, ref in enumerate((vgrad_ref, ggrad_ref, ograd_ref)):
        moves.append((wgrad_in.at[i], wgrad.at[i], ((wgrad.at[i], ref),)))
    ins = [pltpu.make_async_copy(src, dst, in_sem.at[i]) for i, (src, dst, _) in enumerate(moves)]
    for c in ins:
        c.start()
    outs = []
    for c, (_, _, stores) in zip(ins, moves):
        c.wait()
        if len(stores) == 2:
            taps[...] = small[0:tap_count]
            gain[...] = small[tap_count:tap_count + 1]
        for src, dst in stores:
            outs.append(pltpu.make_async_copy(src, dst, out_sem.at[len(outs)]))
            outs[-1].start()
    for c in outs:
        c.wait()


def shards(nsp, ntp, block_input, value_proj, gate_proj, conv_taps, norm_gain, out_proj, grad_output):
    rows, width = block_input.shape
    cl = value_proj.shape[1]
    chan = cl * ntp
    nx = ntp // 2
    ny = nx
    nz = nsp // ny
    nh = nz // 2
    nb_slots = max(nh - 1, 1)
    groups = cl // LANES
    ds = width // nsp
    dt = width // ntp
    nrc = rows // MATMUL_ROWS
    tap_count = conv_taps.shape[0]
    dma = pltpu.SemaphoreType.DMA
    vm = pltpu.VMEM
    wide = vm((groups, rows, LANES), F32)
    padded = vm((groups, rows + PAD, LANES), F32)
    tpad = -(-(tap_count + 1) // 8) * 8
    any_spec = pl.BlockSpec(memory_space=pltpu.HBM)
    vmem_spec = pl.BlockSpec(memory_space=pltpu.VMEM)
    outs = pl.pallas_call(
        functools.partial(kernel, (nsp, ntp, ny, nz, nx, float(chan))),
        out_shape=(
            jax.ShapeDtypeStruct((rows, dt), BF16),
            jax.ShapeDtypeStruct((3, ds, cl), F32),
            jax.ShapeDtypeStruct((tpad, cl), F32),
        ),
        in_specs=[any_spec, any_spec, any_spec, vmem_spec, vmem_spec, any_spec, any_spec],
        out_specs=[vmem_spec] * 3,
        scratch_shapes=[
            vm((rows, width), BF16), vm((width, cl), BF16), vm((width, cl), BF16), vm((width, cl), BF16),
            vm((rows, width), BF16),
            wide, wide, wide, padded, wide, wide, padded,
            vm((rows, cl), BF16), vm((rows, 2 * cl), BF16), vm((rows, 2 * cl), BF16),
            vm((nx, 2, dt, cl), BF16),
            vm((2, 8, LANES), F32), vm((ntp - 1, 2, 8, LANES), F32),
            vm((2, 8, LANES), F32), vm((ntp - 1, 2, 8, LANES), F32),
            vm((nsp, ds, 2 * cl), BF16), vm((nsp, ds, cl), BF16),
            vm((ny - 1, nz, ds, 2 * cl), BF16), vm((ny - 1, nz, ds, cl), BF16),
            vm((nh, ds, 2 * cl), BF16), vm((nh, ds, cl), BF16),
            vm((nh, ds, 2 * cl), BF16), vm((nh, ds, cl), BF16),
            vm((nb_slots, ds, 2 * cl), BF16), vm((nb_slots, ds, cl), BF16),
            vm((nb_slots, ds, 2 * cl), BF16), vm((nb_slots, ds, cl), BF16),
            vm((nx - 1, nrc, MATMUL_ROWS, dt), BF16), vm((nx - 1, nrc, MATMUL_ROWS, dt), BF16),
            vm((tpad, cl), F32), vm((ny - 1, tpad, cl), F32),
            vm((tpad, cl), F32), vm((nz - 1, tpad, cl), F32),
            dma((4 + nrc,)), dma((4,)),
            dma((2, ntp - 1)), dma((2, ntp - 1)),
            dma((nx, 2)), dma((nx, 2)),
            dma((nrc,)), dma((nrc,)),
            dma((nx - 1, nrc)), dma((nx - 1, nrc)),
            dma((2, ny - 1, nz)), dma((2, ny - 1, nz)),
            dma((2, nh)), dma((2, nh)),
            dma((2, nb_slots)), dma((2, nb_slots)),
            dma((ny - 1,)), dma((ny - 1,)),
            dma((nz - 1,)), dma((nz - 1,)),
        ],
        compiler_params=pltpu.CompilerParams(
            collective_id=0, has_side_effects=True, vmem_limit_bytes=60 * 1000 * 1000),
    )(block_input, value_proj, gate_proj, conv_taps, norm_gain.reshape(1, cl), out_proj, grad_output)
    outs = pl.pallas_call(
        hand_out,
        out_shape=(
            jax.ShapeDtypeStruct((rows, dt), BF16),
            jax.ShapeDtypeStruct((ds, cl), F32),
            jax.ShapeDtypeStruct((ds, cl), F32),
            jax.ShapeDtypeStruct((ds, cl), F32),
            jax.ShapeDtypeStruct((tap_count, cl), F32),
            jax.ShapeDtypeStruct((1, cl), F32),
        ),
        in_specs=[any_spec] * 3,
        out_specs=[any_spec] * 6,
        scratch_shapes=[
            vm((rows, dt), BF16), vm((3, ds, cl), F32), vm((tpad, cl), F32),
            vm((tap_count, cl), F32), vm((1, cl), F32),
            dma((4 + nrc,)), dma((5 + nrc,)),
        ],
        compiler_params=pltpu.CompilerParams(vmem_limit_bytes=60 * 1000 * 1000),
    )(*outs)
    return outs[:5] + (outs[5].reshape(cl),)


def solution(mesh):
    return jax.shard_map(
        functools.partial(shards, mesh.shape["sp"], mesh.shape["tp"]),
        mesh=mesh,
        in_specs=(
            P("sp", None),
            P(None, "tp"),
            P(None, "tp"),
            P(None, "tp"),
            P("tp"),
            P(None, "tp"),
            P("sp", None),
        ),
        out_specs=(
            P("sp", "tp"),
            P("sp", "tp"),
            P("sp", "tp"),
            P("sp", "tp"),
            P(None, "tp"),
            P("tp"),
        ),
        check_vma=False,
    )
```

profile of v0, /device:TPU:0, one launch (start us, length us, event | category | flops | bytes accessed | tf_op | source)
XLA Modules:
  0.0 73.1 jit_solution(12928939682767668140)
XLA Ops:
  0.6 70.1 %shard_map.118 = (bf16[1024,512]{1,0:T(8,128)(2,1)}, f32[3,256,256]{2,1,0:T(8,128)}, f32[32,256]{1,0:T(8,128)}) custom-call(bf16[1024,2048]{1,0:T(8,128)(2,1)} %bi_hbm.1, bf16[2048,256]{1,0:T(8,128)(2,1)} %wv_hbm.1, bf16[2048,256]{1,0:T(8,128)(2,1)} %wg_hbm.1, f32[31,256]{1,0:T(8,128)} %taps_ref.1, f32[1,256]{1,0:T(1,128)} %bitcast.2, ...), custom_call_target="tpu_custom_call" | custom-call | tf_op jit(solution)/shard_map/pallas_call | solution.py:519
  70.7 2.3 %shard_map.119 = (bf16[1024,512]{1,0:T(8,128)(2,1)}, f32[256,256]{1,0:T(8,128)}, f32[256,256]{1,0:T(8,128)}, f32[256,256]{1,0:T(8,128)}, f32[31,256]{1,0:T(8,128)}, /*index=5*/f32[1,256]{1,0:T(1,128)}) custom-call(bf16[1024,512]{1,0:T(8,128)(2,1)} %get-tuple-element.15.ig_in, f32[3,256,256]{2,1,0:T(8,128)} %get-tuple-element.16.wgrad_in, ...), custom_call_target="tpu_custom_call" | custom-call | tf_op jit(solution)/shard_map/pallas_call | solution.py:559
where the time goes:
time: 73.3 us; the launch traced here: 73.1 us
  Pallas kernels  72.4 us (99%)
    pallas_call x1, Pallas kernels, shards(): pl.pallas_call(functools.partial(kernel, (nsp, ntp, ny, nz, nx, float(cha...  70.1 us
    pallas_call x1, Pallas kernels, shards(): pl.pallas_call(hand_out, out_shape=(jax.ShapeDtypeStruct((rows, dt), BF16...  2.34 us

commit v1 on v0

--- a/solution.py
+++ b/solution.py
@@ -251,16 +251,18 @@
         for j in range(per):
             dst[chunk * per + j] = t[j * ds:(j + 1) * ds]
 
-    def weight_peer_part(src, right, dst, copies):
+    def weight_peer_part(src, right, dst, copies, send=True):
         if per == 1:
             for o, r in peers:
                 weight_chunk(src, right, dst, plane(o) * ny + wrap(y + r, ny))
-                copies[o, r].start()
+                if send:
+                    copies[o, r].start()
         else:
             for chunk in range(nsp // per):
                 weight_chunk(src, right, dst, chunk)
             for o, r in peers:
-                copies[o, r].start()
+                if send:
+                    copies[o, r].start()
 
     def weight_own_part(src, right, dst):
         if per == 1:
@@ -269,7 +271,7 @@
 
     yc_out = y_copies(0, gout, yout)
     yc_vg = y_copies(1, gvg, yvg)
-    weight_peer_part(go, act, gout, yc_out)
+    weight_peer_part(go, act, gout, yc_out, send=False)
 
     for c in st_copies:
         c.wait()
@@ -293,6 +295,9 @@
     @pl.when(has_prev)
     def _():
         back.start()
+
+    for o, r in peers:
+        yc_out[o, r].start()
 
     lax.fori_loop(1, nb, slope_block, 0)
 

time: 73.3 us -> 68.7 us (0.937)
  Pallas kernels: 72.4 us -> 67.8 us
    pallas_call x1, Pallas kernels: 70.1 us -> 65.5 us  [shards(): pl.pallas_call(functools.partial(kernel, (nsp, ntp, ny, nz, nx, float(cha...]
where the time goes in v1:
time: 68.7 us; the launch traced here: 68.4 us
  Pallas kernels  67.8 us (99%)
    pallas_call x1, Pallas kernels, shards(): pl.pallas_call(functools.partial(kernel, (nsp, ntp, ny, nz, nx, float(cha...  65.5 us
    pallas_call x1, Pallas kernels, shards(): pl.pallas_call(hand_out, out_shape=(jax.ShapeDtypeStruct((rows, dt), BF16...  2.34 us

profile of v1, /device:TPU:0, one launch (start us, length us, event | category | flops | bytes accessed | tf_op | source)
XLA Modules:
  0.0 68.4 jit_solution(7798312496972622735)
XLA Ops:
  0.6 65.5 %shard_map.118 = (bf16[1024,512]{1,0:T(8,128)(2,1)}, f32[3,256,256]{2,1,0:T(8,128)}, f32[32,256]{1,0:T(8,128)}) custom-call(bf16[1024,2048]{1,0:T(8,128)(2,1)} %bi_hbm.1, bf16[2048,256]{1,0:T(8,128)(2,1)} %wv_hbm.1, bf16[2048,256]{1,0:T(8,128)(2,1)} %wg_hbm.1, f32[31,256]{1,0:T(8,128)} %taps_ref.1, f32[1,256]{1,0:T(1,128)} %bitcast.2, ...), custom_call_target="tpu_custom_call" | custom-call | tf_op jit(solution)/shard_map/pallas_call | solution.py:524
  66.1 2.3 %shard_map.119 = (bf16[1024,512]{1,0:T(8,128)(2,1)}, f32[256,256]{1,0:T(8,128)}, f32[256,256]{1,0:T(8,128)}, f32[256,256]{1,0:T(8,128)}, f32[31,256]{1,0:T(8,128)}, /*index=5*/f32[1,256]{1,0:T(1,128)}) custom-call(bf16[1024,512]{1,0:T(8,128)(2,1)} %get-tuple-element.15.ig_in, f32[3,256,256]{2,1,0:T(8,128)} %get-tuple-element.16.wgrad_in, ...), custom_call_target="tpu_custom_call" | custom-call | tf_op jit(solution)/shard_map/pallas_call | solution.py:564

commit v2 on v0

--- a/solution.py
+++ b/solution.py
@@ -25,10 +25,10 @@
     return lax.dot_general(a, b, (((0,), (0,)), ((), ())), preferred_element_type=F32)
 
 
-def kernel(cfg, bi_hbm, wv_hbm, wg_hbm, taps_ref, gain_ref, wo_hbm, go_hbm,
-           ig_ref, wgrad_ref, small_ref,
-           bi, wv, wg, wo, go, val, sg, slope, hist, nrm, nsl, fut, act, sl, psl, pw,
-           st1, st1r, st2, st2r, gvg, gout, yvg, yout, avg, aout, arvg, arout, bvg, bout, brvg, brout,
+def kernel(cfg, bi_hbm, wv_hbm, wg_hbm, taps_hbm, gain_hbm, wo_hbm, go_hbm,
+           ig_ref, wgrad_ref, tgrad_ref, gaingrad_ref,
+           bi, wv, wg, wo, go, taps_ref, gain_ref, val, sg, slope, hist, nrm, nsl, fut, act, sl, psl, pw,
+           st1, st1r, st2, st2r, spa, spb, gb, yb, ab, ar, bb, br,
            xs, xr, tg, tgy, tgz, tgzr,
            ld_sem, halo_sem, st_send, st_recv, pw_send, pw_recv, sl_send, sl_recv,
            x_send, x_recv, y_send, y_recv, a_send, a_recv, b_send, b_recv, ty_send, ty_recv, tz_send, tz_recv):
@@ -64,8 +64,10 @@
     for n, i in enumerate(reversed(range(nrc))):
         s = pl.ds(i * MATMUL_ROWS, MATMUL_ROWS)
         load("bi%d" % i, bi_hbm.at[s], bi.at[s], 2 + n)
-    load("wo", wo_hbm, wo, 2 + nrc)
-    load("go", go_hbm, go, 3 + nrc)
+    load("taps", taps_hbm, taps_ref, 2 + nrc)
+    load("gain", gain_hbm, gain_ref, 3 + nrc)
+    load("wo", wo_hbm, wo, 4 + nrc)
+    load("go", go_hbm, go, 5 + nrc)
 
     barrier = pltpu.get_barrier_semaphore()
     for o in range(1, nsp):
@@ -132,11 +134,19 @@
             packed = jnp.where(lane == b * vpb + i, red[8 * i:8 * i + 8], packed)
         return packed
 
-    def unpack(rolled):
-        return jnp.concatenate([rolled[:, i:i + 1] for i in range(vpb)], axis=0)
-
-    def roll_to(packed, b):
-        return pltpu.roll(packed, lax.rem(LANES - b * vpb, LANES), 1)
+    ahead = (lax.broadcasted_iota(jnp.int32, (ROW_BLOCK, LANES), 1)
+             - lax.broadcasted_iota(jnp.int32, (ROW_BLOCK, LANES), 0) // 8)
+    ones = jnp.ones((3 * LANES, LANES), BF16)
+
+    def spread(packed, dst):
+        high = packed.astype(BF16).astype(F32)
+        rest = packed - high
+        mid = rest.astype(BF16).astype(F32)
+        parts = [jnp.concatenate([p] * vpb, axis=0) for p in (high, mid, rest - mid)]
+        for b in range(nb):
+            own = ahead == b * vpb
+            t = jnp.concatenate([jnp.where(own, p, 0.0).astype(BF16) for p in parts], axis=1)
+            dst[b * ROW_BLOCK:(b + 1) * ROW_BLOCK, :] = jnp.dot(t, ones, preferred_element_type=F32)
 
     def tap(k, g):
         return taps_ref[k:k + 1, g * LANES:(g + 1) * LANES]
@@ -155,6 +165,8 @@
                 pack(psq, jnp.sum(q, axis=1, keepdims=True), b))
 
     zero = jnp.zeros((8, LANES), F32)
+    loads["taps"].wait()
+    loads["gain"].wait()
     carry = lax.fori_loop(0, nb - 1, lambda i, c: conv_block(nb - 1 - i, c), (zero, zero))
 
     @pl.when(has_prev)
@@ -193,11 +205,14 @@
     center = tsum / chan
     inverse = lax.rsqrt(tsq / chan - center * center + NORM_FLOOR)
 
+    spread(center, spa)
+    spread(inverse, spb)
+
     def norm_block(b, carry):
         psum, pcross, gacc = carry
         r = pl.ds(pl.multiple_of(b * ROW_BLOCK, ROW_BLOCK), ROW_BLOCK)
-        cen = unpack(roll_to(center, b))
-        inv = unpack(roll_to(inverse, b))
+        cen = spa[r, :]
+        inv = spb[r, :]
         s = q = None
         gout_acc = []
         for g in range(groups):
@@ -237,39 +252,47 @@
 
     peers = [(u, r) for u in range(nz) for r in range(1, ny)]
 
-    def y_copies(which, src, dst):
-        out = {}
+    y_copies = {}
+    for which in range(3):
         for o, r in peers:
             yy = wrap(y + r, ny)
-            out[o, r] = remote(src.at[plane(o) * ny + yy], dst.at[r - 1, o], y_send.at[which, r - 1, o],
-                               y_recv.at[which, r - 1, o], {"sp": z * ny + yy})
-        return out
-
-    def weight_chunk(src, right, dst, chunk):
+            y_copies[which, o, r] = remote(gb.at[which, plane(o) * ny + yy], yb.at[which, r - 1, o],
+                                           y_send.at[which, r - 1, o], y_recv.at[which, r - 1, o],
+                                           {"sp": z * ny + yy})
+
+    def y_start(which, o):
+        for r in range(1, ny):
+            y_copies[which, o, r].start()
+
+    def weight_chunk(src, right, first, count, chunk):
         cols = pl.ds(pl.multiple_of(chunk * per * ds, per * ds), per * ds)
         t = dot_tn(src[:, cols], right[...]).astype(BF16)
         for j in range(per):
-            dst[chunk * per + j] = t[j * ds:(j + 1) * ds]
-
-    def weight_peer_part(src, right, dst, copies):
+            for n in range(count):
+                gb[first + n, chunk * per + j] = t[j * ds:(j + 1) * ds, n * cl:(n + 1) * cl]
+
+    def weight_peer_part(src, right, first, count, started):
         if per == 1:
-            for o, r in peers:
-                weight_chunk(src, right, dst, plane(o) * ny + wrap(y + r, ny))
-                copies[o, r].start()
+            for o in range(nz):
+                for r in range(1, ny):
+                    weight_chunk(src, right, first, count, plane(o) * ny + wrap(y + r, ny))
+                started(o)
         else:
             for chunk in range(nsp // per):
-                weight_chunk(src, right, dst, chunk)
-            for o, r in peers:
-                copies[o, r].start()
-
-    def weight_own_part(src, right, dst):
+                weight_chunk(src, right, first, count, chunk)
+            for o in range(nz):
+                started(o)
+
+    def weight_own_part(src, right, first, count):
         if per == 1:
             for o in range(nz):
-                weight_chunk(src, right, dst, plane(o) * ny + y)
-
-    yc_out = y_copies(0, gout, yout)
-    yc_vg = y_copies(1, gvg, yvg)
-    weight_peer_part(go, act, gout, yc_out)
+                weight_chunk(src, right, first, count, plane(o) * ny + y)
+
+    def out_started(o):
+        if o == 0:
+            y_start(2, 0)
+
+    weight_peer_part(go, act, 2, 1, out_started)
 
     for c in st_copies:
         c.wait()
@@ -280,10 +303,13 @@
     tsum = tsum / chan * inverse
     tcross = tcross / chan * inverse
 
+    spread(tsum, spa)
+    spread(tcross, spb)
+
     def slope_block(b, c):
         r = pl.ds(pl.multiple_of(b * ROW_BLOCK, ROW_BLOCK), ROW_BLOCK)
-        ss = unpack(roll_to(tsum, b))
-        cs = unpack(roll_to(tcross, b))
+        ss = spa[r, :]
+        cs = spb[r, :]
         for g in range(groups):
             fut[g, r, :] = nsl[g, r, :] - ss - nrm[g, r, :] * cs
         return c
@@ -293,6 +319,9 @@
     @pl.when(has_prev)
     def _():
         back.start()
+
+    for o in range(1, nz):
+        y_start(2, o)
 
     lax.fori_loop(1, nb, slope_block, 0)
 
@@ -348,55 +377,60 @@
         if i > 0:
             input_send(i - 1)
 
-    weight_peer_part(bi, sl, gvg, yc_vg)
+    def vg_started(o):
+        if o == nz - 1 or (o == nz - 2 and nh > 1):
+            if o == nz - 2:
+                y_start(0, o)
+                y_start(1, o)
+        elif o % 2 == 1:
+            for which in range(2):
+                y_start(which, o - 1)
+                y_start(which, o)
+
+    weight_peer_part(bi, sl, 0, 2, vg_started)
     input_send(nrc - 1)
 
-    weight_own_part(go, act, gout)
-    weight_own_part(bi, sl, gvg)
-
-    def y_sum(u, gb, yb, ycs):
-        t = gb[plane(u) * ny + y].astype(F32)
+    weight_own_part(go, act, 2, 1)
+
+    def y_sum(which, u):
+        t = gb[which, plane(u) * ny + y].astype(F32)
         for r in range(1, ny):
-            ycs[u, r].wait()
-            t = t + yb[r - 1, u].astype(F32)
+            y_copies[which, u, r].wait()
+            t = t + yb[which, r - 1, u].astype(F32)
         return t
 
     pair = {"sp": (2 * zh + 1 - zl) * ny + y}
     across = {}
 
     def a_step(which, h):
-        gb, yb, ycs, buf, rbuf = ((gout, yout, yc_out, aout, arout), (gvg, yvg, yc_vg, avg, arvg))[which]
-        buf[h] = y_sum(2 * h, gb, yb, ycs).astype(BF16)
-        c = remote(buf.at[h], rbuf.at[h], a_send.at[which, h], a_recv.at[which, h], pair)
+        ab[which, h] = y_sum(which, 2 * h).astype(BF16)
+        c = remote(ab.at[which, h], ar.at[which, h], a_send.at[which, h], a_recv.at[which, h], pair)
         c.start()
         across[which, h] = c
 
     def b_sum(which, h):
-        gb, yb, ycs, rbuf = ((gout, yout, yc_out, arout), (gvg, yvg, yc_vg, arvg))[which]
-        t = y_sum(2 * h + 1, gb, yb, ycs)
+        t = y_sum(which, 2 * h + 1)
         across[which, h].wait()
-        return t + rbuf[h].astype(F32)
+        return t + ar[which, h].astype(F32)
 
     b_copies = {}
 
     def b_step(which, h):
-        buf, rbuf = ((bout, brout), (bvg, brvg))[which]
-        buf[h] = b_sum(which, h).astype(BF16)
-        c = remote(buf.at[h], rbuf.at[h], b_send.at[which, h], b_recv.at[which, h],
+        bb[which, h] = b_sum(which, h).astype(BF16)
+        c = remote(bb.at[which, h], br.at[which, h], b_send.at[which, h], b_recv.at[which, h],
                    {"sp": (2 * wrap(zh + h + 1, nh) + zl) * ny + y})
         c.start()
         b_copies[which, h] = c
 
     def final_sum(which):
-        rbuf = (brout, brvg)[which]
         t = b_sum(which, nh - 1)
         for h in range(nh - 1):
             b_copies[which, h].wait()
-            t = t + rbuf[h].astype(F32)
-        return t
+            t = t + br[which, h].astype(F32)
+        wgrad_ref[which] = t
 
     for h in range(nh):
-        a_step(0, h)
+        a_step(2, h)
 
     step = 4
     for g in range(groups):
@@ -423,9 +457,18 @@
         c.start()
         tzc.append(c)
 
+    weight_own_part(bi, sl, 0, 2)
+
     for h in range(nh - 1):
-        b_step(0, h)
-    a_step(1, 0)
+        b_step(2, h)
+
+    def first_part(which, h):
+        a_step(which, h)
+        if h < nh - 1:
+            b_step(which, h)
+
+    if nh > 1:
+        a_step(0, 0)
     t = tg[...]
     for o in range(1, nz):
         tzc[o - 1].wait()
@@ -436,29 +479,36 @@
         c = remote(tgz, tgy.at[r - 1], ty_send.at[r - 1], ty_recv.at[r - 1], {"sp": z * ny + wrap(y + r, ny)})
         c.start()
         tyc.append(c)
+    for o in range(nz - 1 if nh > 1 else nz - 2, nz):
+        y_start(0, o)
+        y_start(1, o)
     for h in range(nh - 1):
+        if h > 0:
+            a_step(0, h)
+        b_step(0, h)
+        a_step(1, h)
         b_step(1, h)
-        a_step(1, h + 1)
-
-    wgrad_ref[2] = final_sum(0)
-
-    for i in range(nrc):
+
+    def input_own(i):
         t = input_part(i, x)
         for o in range(1, nx):
             xc[i * (nx - 1) + o - 1].wait()
             t = t + xr[o - 1, i].astype(F32)
         ig_ref[i * MATMUL_ROWS:(i + 1) * MATMUL_ROWS, :] = t.astype(BF16)
 
-
-    own = final_sum(1)
-    wgrad_ref[0] = own[:, 0:cl]
-    wgrad_ref[1] = own[:, cl:2 * cl]
-
+    a_step(0, nh - 1)
+    a_step(1, nh - 1)
+    final_sum(2)
+    for i in range(nrc):
+        input_own(i)
     t = tgz[...]
     for r in range(1, ny):
         tyc[r - 1].wait()
         t = t + tgy[r - 1]
-    small_ref[...] = t
+    tgrad_ref[...] = t[0:tap_count]
+    gaingrad_ref[...] = t[tap_count:tap_count + 1]
+    final_sum(0)
+    final_sum(1)
 
     @pl.when(has_next)
     def _():
@@ -469,29 +519,13 @@
         back.wait_send()
 
 
-def hand_out(ig_in, wgrad_in, small_in, ig_ref, vgrad_ref, ggrad_ref, ograd_ref, tgrad_ref, gaingrad_ref,
-             ig, wgrad, small, taps, gain, in_sem, out_sem):
-    tap_count = tgrad_ref.shape[0]
-    parts = ig.shape[0] // MATMUL_ROWS
-    moves = [(small_in, small, ((taps, tgrad_ref), (gain, gaingrad_ref)))]
-    for i in range(parts):
-        s = pl.ds(i * MATMUL_ROWS, MATMUL_ROWS)
-        moves.append((ig_in.at[s], ig.at[s], ((ig.at[s], ig_ref.at[s]),)))
-    for i, ref in enumerate((vgrad_ref, ggrad_ref, ograd_ref)):
-        moves.append((wgrad_in.at[i], wgrad.at[i], ((wgrad.at[i], ref),)))
-    ins = [pltpu.make_async_copy(src, dst, in_sem.at[i]) for i, (src, dst, _) in enumerate(moves)]
-    for c in ins:
+def hand_out(ig, wgrad, taps, gain, ig_ref, vgrad_ref, ggrad_ref, ograd_ref, tgrad_ref, gaingrad_ref, out_sem):
+    moves = [(wgrad.at[i], ref) for i, ref in enumerate((vgrad_ref, ggrad_ref, ograd_ref))]
+    moves += [(ig, ig_ref), (taps, tgrad_ref), (gain, gaingrad_ref)]
+    copies = [pltpu.make_async_copy(src, dst, out_sem.at[i]) for i, (src, dst) in enumerate(moves)]
+    for c in copies:
         c.start()
-    outs = []
-    for c, (_, _, stores) in zip(ins, moves):
-        c.wait()
-        if len(stores) == 2:
-            taps[...] = small[0:tap_count]
-            gain[...] = small[tap_count:tap_count + 1]
-        for src, dst in stores:
-            outs.append(pltpu.make_async_copy(src, dst, out_sem.at[len(outs)]))
-            outs[-1].start()
-    for c in outs:
+    for c in copies:
         c.wait()
 
 
@@ -521,41 +555,42 @@
         out_shape=(
             jax.ShapeDtypeStruct((rows, dt), BF16),
             jax.ShapeDtypeStruct((3, ds, cl), F32),
-            jax.ShapeDtypeStruct((tpad, cl), F32),
+            jax.ShapeDtypeStruct((tap_count, cl), F32),
+            jax.ShapeDtypeStruct((1, cl), F32),
         ),
-        in_specs=[any_spec, any_spec, any_spec, vmem_spec, vmem_spec, any_spec, any_spec],
-        out_specs=[vmem_spec] * 3,
+        in_specs=[any_spec] * 7,
+        out_specs=[vmem_spec] * 4,
         scratch_shapes=[
             vm((rows, width), BF16), vm((width, cl), BF16), vm((width, cl), BF16), vm((width, cl), BF16),
             vm((rows, width), BF16),
+            vm((tap_count, cl), F32), vm((1, cl), F32),
             wide, wide, wide, padded, wide, wide, padded,
             vm((rows, cl), BF16), vm((rows, 2 * cl), BF16), vm((rows, 2 * cl), BF16),
             vm((nx, 2, dt, cl), BF16),
             vm((2, 8, LANES), F32), vm((ntp - 1, 2, 8, LANES), F32),
             vm((2, 8, LANES), F32), vm((ntp - 1, 2, 8, LANES), F32),
-            vm((nsp, ds, 2 * cl), BF16), vm((nsp, ds, cl), BF16),
-            vm((ny - 1, nz, ds, 2 * cl), BF16), vm((ny - 1, nz, ds, cl), BF16),
-            vm((nh, ds, 2 * cl), BF16), vm((nh, ds, cl), BF16),
-            vm((nh, ds, 2 * cl), BF16), vm((nh, ds, cl), BF16),
-            vm((nb_slots, ds, 2 * cl), BF16), vm((nb_slots, ds, cl), BF16),
-            vm((nb_slots, ds, 2 * cl), BF16), vm((nb_slots, ds, cl), BF16),
+            vm((rows, LANES), F32), vm((rows, LANES), F32),
+            vm((3, nsp, ds, cl), BF16), vm((3, ny - 1, nz, ds, cl), BF16),
+            vm((3, nh, ds, cl), BF16), vm((3, nh, ds, cl), BF16),
+            vm((3, nb_slots, ds, cl), BF16), vm((3, nb_slots, ds, cl), BF16),
             vm((nx - 1, nrc, MATMUL_ROWS, dt), BF16), vm((nx - 1, nrc, MATMUL_ROWS, dt), BF16),
             vm((tpad, cl), F32), vm((ny - 1, tpad, cl), F32),
             vm((tpad, cl), F32), vm((nz - 1, tpad, cl), F32),
-            dma((4 + nrc,)), dma((4,)),
+            dma((6 + nrc,)), dma((4,)),
             dma((2, ntp - 1)), dma((2, ntp - 1)),
             dma((nx, 2)), dma((nx, 2)),
             dma((nrc,)), dma((nrc,)),
             dma((nx - 1, nrc)), dma((nx - 1, nrc)),
-            dma((2, ny - 1, nz)), dma((2, ny - 1, nz)),
-            dma((2, nh)), dma((2, nh)),
-            dma((2, nb_slots)), dma((2, nb_slots)),
+            dma((3, ny - 1, nz)), dma((3, ny - 1, nz)),
+            dma((3, nh)), dma((3, nh)),
+            dma((3, nb_slots)), dma((3, nb_slots)),
             dma((ny - 1,)), dma((ny - 1,)),
             dma((nz - 1,)), dma((nz - 1,)),
         ],
         compiler_params=pltpu.CompilerParams(
-            collective_id=0, has_side_effects=True, vmem_limit_bytes=60 * 1000 * 1000),
-    )(block_input, value_proj, gate_proj, conv_taps, norm_gain.reshape(1, cl), out_proj, grad_output)
+            collective_id=0, has_side_effects=True, vmem_limit_bytes=46 * 1000 * 1000),
+    )(*[pltpu.with_memory_space_constraint(a, pltpu.HBM) for a in (
+        block_input, value_proj, gate_proj, conv_taps, norm_gain.reshape(1, cl), out_proj, grad_output)])
     outs = pl.pallas_call(
         hand_out,
         out_shape=(
@@ -566,14 +601,10 @@
             jax.ShapeDtypeStruct((tap_count, cl), F32),
             jax.ShapeDtypeStruct((1, cl), F32),
         ),
-        in_specs=[any_spec] * 3,
+        in_specs=[vmem_spec] * 4,
         out_specs=[any_spec] * 6,
-        scratch_shapes=[
-            vm((rows, dt), BF16), vm((3, ds, cl), F32), vm((tpad, cl), F32),
-            vm((tap_count, cl), F32), vm((1, cl), F32),
-            dma((4 + nrc,)), dma((5 + nrc,)),
-        ],
-        compiler_params=pltpu.CompilerParams(vmem_limit_bytes=60 * 1000 * 1000),
+        scratch_shapes=[dma((6,))],
+        compiler_params=pltpu.CompilerParams(vmem_limit_bytes=8 * 1000 * 1000),
     )(*outs)
     return outs[:5] + (outs[5].reshape(cl),)
 

time: 73.3 us -> 61.7 us (0.84)
  Pallas kernels: 72.4 us -> 60.8 us
    pallas_call x1, Pallas kernels: 70.1 us -> 59.5 us  [shards(): pl.pallas_call(functools.partial(kernel, (nsp, ntp, ny, nz, nx, float(cha...]
    pallas_call x1, Pallas kernels: 2.34 us -> 1.29 us  [shards(): pl.pallas_call(hand_out, out_shape=(jax.ShapeDtypeStruct((rows, dt), BF16...]
where the time goes in v2:
time: 61.7 us; the launch traced here: 61.6 us
  Pallas kernels  60.8 us (99%)
  between operations  0.8 us (1%)
    pallas_call x1, Pallas kernels, shards(): pl.pallas_call(functools.partial(kernel, (nsp, ntp, ny, nz, nx, float(cha...  59.5 us
    pallas_call x1, Pallas kernels, shards(): pl.pallas_call(hand_out, out_shape=(jax.ShapeDtypeStruct((rows, dt), BF16...  1.29 us

profile of v2, /device:TPU:0, one launch (start us, length us, event | category | flops | bytes accessed | tf_op | source)
XLA Modules:
  0.0 61.6 jit_solution(2857359476643945239)
XLA Ops:
  0.6 59.5 %shard_map.118 = (bf16[1024,512]{1,0:T(8,128)(2,1)S(1)}, f32[3,256,256]{2,1,0:T(8,128)S(1)}, f32[31,256]{1,0:T(8,128)S(1)}, f32[1,256]{1,0:T(1,128)S(1)}) custom-call(bf16[1024,2048]{1,0:T(8,128)(2,1)} %bi_hbm.1, bf16[2048,256]{1,0:T(8,128)(2,1)} %wv_hbm.1, bf16[2048,256]{1,0:T(8,128)(2,1)} %wg_hbm.1, f32[31,256]{1,0:T(8,128)} %taps_hbm.1, ...), custom_call_target="tpu_custom_call" | custom-call | tf_op jit(solution)/shard_map/pallas_call | solution.py:553
  60.1 1.3 %shard_map.119 = (bf16[1024,512]{1,0:T(8,128)(2,1)}, f32[256,256]{1,0:T(8,128)}, f32[256,256]{1,0:T(8,128)}, f32[256,256]{1,0:T(8,128)}, f32[31,256]{1,0:T(8,128)}, /*index=5*/f32[1,256]{1,0:T(1,128)}) custom-call(bf16[1024,512]{1,0:T(8,128)(2,1)S(1)} %get-tuple-element.16.ig, f32[3,256,256]{2,1,0:T(8,128)S(1)} %get-tuple-element.17.wgrad, ...), custom_call_target="tpu_custom_call" | custom-call | tf_op jit(solution)/shard_map/pallas_call | solution.py:594

commit v3 on v2

--- a/solution.py
+++ b/solution.py
@@ -28,10 +28,10 @@
 def kernel(cfg, bi_hbm, wv_hbm, wg_hbm, taps_hbm, gain_hbm, wo_hbm, go_hbm,
            ig_ref, wgrad_ref, tgrad_ref, gaingrad_ref,
            bi, wv, wg, wo, go, taps_ref, gain_ref, val, sg, slope, hist, nrm, nsl, fut, act, sl, psl, pw,
-           st1, st1r, st2, st2r, spa, spb, gb, yb, ab, ar, bb, br,
+           st1, st1r, st2, st2r, spa, spb, gb, yb, zb, zin,
            xs, xr, tg, tgy, tgz, tgzr,
            ld_sem, halo_sem, st_send, st_recv, pw_send, pw_recv, sl_send, sl_recv,
-           x_send, x_recv, y_send, y_recv, a_send, a_recv, b_send, b_recv, ty_send, ty_recv, tz_send, tz_recv):
+           x_send, x_recv, y_send, y_recv, z_send, z_recv, ty_send, ty_recv, tz_send, tz_recv):
     nsp, ntp, ny, nz, nx, chan = cfg
     rows, width = bi.shape
     cl = wv.shape[1]
@@ -106,27 +106,6 @@
     def _():
         fut[:, rows:rows + PAD, :] = jnp.zeros((groups, PAD, LANES), F32)
 
-    loads["wv"].wait()
-    loads["wg"].wait()
-    partner = {"tp": 2 * x + 1 - core}
-    pws = []
-    for n, i in enumerate(reversed(range(nrc))):
-        loads["bi%d" % i].wait()
-        glu(i)
-        if n == 0:
-            pl.semaphore_wait(barrier, nsp + ntp - 2)
-
-            @pl.when(has_next)
-            def _():
-                halo.start()
-
-            for xx in range(nx):
-                for j, w in enumerate((wv, wg)):
-                    first = pl.multiple_of((2 * xx + 1 - core) * dt, dt)
-                    c = remote(w.at[pl.ds(first, dt), :], pw.at[xx, j], pw_send.at[xx, j], pw_recv.at[xx, j], partner)
-                    c.start()
-                    pws.append(c)
-
     lane = lax.broadcasted_iota(jnp.int32, (8, LANES), 1)
 
     def pack(packed, red, b):
@@ -165,9 +144,39 @@
                 pack(psq, jnp.sum(q, axis=1, keepdims=True), b))
 
     zero = jnp.zeros((8, LANES), F32)
-    loads["taps"].wait()
-    loads["gain"].wait()
-    carry = lax.fori_loop(0, nb - 1, lambda i, c: conv_block(nb - 1 - i, c), (zero, zero))
+    loads["wv"].wait()
+    loads["wg"].wait()
+    partner = {"tp": 2 * x + 1 - core}
+    pws = []
+    bpc = MATMUL_ROWS // ROW_BLOCK
+    carry = (zero, zero)
+    for n, i in enumerate(reversed(range(nrc))):
+        if n == 0:
+            loads["bi%d" % i].wait()
+        else:
+            for b in reversed(range(max(i * bpc + bpc + 1, 0), min(i * bpc + 2 * bpc + 1, nb))):
+                carry = conv_block(b, carry)
+        glu(i)
+        if n == 0:
+            loads["taps"].wait()
+            loads["gain"].wait()
+            for j in reversed(range(nrc - 1)):
+                loads["bi%d" % j].wait()
+            pl.semaphore_wait(barrier, nsp + ntp - 2)
+
+            @pl.when(has_next)
+            def _():
+                halo.start()
+
+            for xx in range(nx):
+                for j, w in enumerate((wv, wg)):
+                    first = pl.multiple_of((2 * xx + 1 - core) * dt, dt)
+                    c = remote(w.at[pl.ds(first, dt), :], pw.at[xx, j], pw_send.at[xx, j], pw_recv.at[xx, j], partner)
+                    c.start()
+                    pws.append(c)
+
+    for b in reversed(range(1, bpc + 1)):
+        carry = conv_block(b, carry)
 
     @pl.when(has_prev)
     def _():
@@ -242,13 +251,15 @@
     st_copies = share(1, st2, st2r)
 
     per = max(1, min(256, width) // ds)
-    zh = z // 2
-    zl = z % 2
-    nh = nz // 2
+    low = z < nz // 2
+    reach = jnp.where(low, nz - 1 - z, z)
 
     def plane(u):
-        side = zl if u % 2 else 1 - zl
-        return 2 * wrap(zh + u // 2 + 1, nh) + side
+        if u == nz - 1:
+            return z
+        up = jnp.where(low, nz - 1 - u, u)
+        down = jnp.where(low, u - reach, nz - 1 - (u - reach))
+        return jnp.where(u < reach, up, down)
 
     peers = [(u, r) for u in range(nz) for r in range(1, ny)]
 
@@ -283,16 +294,64 @@
             for o in range(nz):
                 started(o)
 
-    def weight_own_part(src, right, first, count):
+    def weight_own_part(src, right, first, count, planes):
         if per == 1:
-            for o in range(nz):
+            for o in planes:
                 weight_chunk(src, right, first, count, plane(o) * ny + y)
+
+    def y_sum(which, u):
+        t = gb[which, plane(u) * ny + y].astype(F32)
+        for r in range(1, ny):
+            y_copies[which, u, r].wait()
+            t = t + yb[which, r - 1, u].astype(F32)
+        return t
+
+    def chain_in(which, slot):
+        return remote(zin.at[which, slot], zin.at[which, slot], z_send.at[which, 0], z_recv.at[which, slot],
+                      {"sp": wrap(z + 1, nz) * ny + y})
+
+    edge = jnp.logical_or(z == 0, z == nz - 1)
+
+    def chain_copy(which, u):
+        p = plane(u)
+        right = p > z
+        slot = jnp.where(p == z - 1, nz, p)
+        return remote(zb.at[which, u], zin.at[which, slot], z_send.at[which, u], z_recv.at[which, slot],
+                      {"sp": jnp.where(right, z + 1, z - 1) * ny + y})
+
+    def edge_step(which, u):
+        @pl.when(edge)
+        def _():
+            zb[which, u] = y_sum(which, u).astype(BF16)
+            chain_copy(which, u).start()
+
+    def middle_step(which, u):
+        @pl.when(jnp.logical_not(edge))
+        def _():
+            t = y_sum(which, u)
+            chain_in(which, plane(u)).wait_recv()
+            zb[which, u] = (t + zin[which, plane(u)].astype(F32)).astype(BF16)
+            chain_copy(which, u).start()
+
+    def final_sum(which):
+        wgrad_ref[which] = y_sum(which, nz - 1)
+
+        @pl.when(z > 0)
+        def _():
+            chain_in(which, z).wait_recv()
+            wgrad_ref[which] = wgrad_ref[which] + zin[which, z].astype(F32)
+
+        @pl.when(z < nz - 1)
+        def _():
+            chain_in(which, nz).wait_recv()
+            wgrad_ref[which] = wgrad_ref[which] + zin[which, nz].astype(F32)
 
     def out_started(o):
         if o == 0:
             y_start(2, 0)
 
     weight_peer_part(go, act, 2, 1, out_started)
+    weight_own_part(go, act, 2, 1, (0,))
 
     for c in st_copies:
         c.wait()
@@ -357,7 +416,6 @@
 
     for c in pws:
         c.wait()
-    bpc = MATMUL_ROWS // ROW_BLOCK
     slc = []
     for i in range(nrc):
         if i == nrc - 1:
@@ -376,62 +434,27 @@
         slc.append(c)
         if i > 0:
             input_send(i - 1)
+        if i == 1:
+            edge_step(2, 0)
+        if i == 2:
+            weight_own_part(go, act, 2, 1, range(1, nz - 2))
 
     def vg_started(o):
-        if o == nz - 1 or (o == nz - 2 and nh > 1):
-            if o == nz - 2:
-                y_start(0, o)
-                y_start(1, o)
-        elif o % 2 == 1:
+        if o == nz - 2:
+            y_start(0, o)
+            y_start(1, o)
+        elif o < nz - 2 and (o % 2 == 1 or o == nz - 3):
             for which in range(2):
-                y_start(which, o - 1)
-                y_start(which, o)
-
+                for v in range(o - o % 2, o + 1):
+                    y_start(which, v)
+
+    for u in range(1, nz - 2):
+        edge_step(2, u)
     weight_peer_part(bi, sl, 0, 2, vg_started)
     input_send(nrc - 1)
-
-    weight_own_part(go, act, 2, 1)
-
-    def y_sum(which, u):
-        t = gb[which, plane(u) * ny + y].astype(F32)
-        for r in range(1, ny):
-            y_copies[which, u, r].wait()
-            t = t + yb[which, r - 1, u].astype(F32)
-        return t
-
-    pair = {"sp": (2 * zh + 1 - zl) * ny + y}
-    across = {}
-
-    def a_step(which, h):
-        ab[which, h] = y_sum(which, 2 * h).astype(BF16)
-        c = remote(ab.at[which, h], ar.at[which, h], a_send.at[which, h], a_recv.at[which, h], pair)
-        c.start()
-        across[which, h] = c
-
-    def b_sum(which, h):
-        t = y_sum(which, 2 * h + 1)
-        across[which, h].wait()
-        return t + ar[which, h].astype(F32)
-
-    b_copies = {}
-
-    def b_step(which, h):
-        bb[which, h] = b_sum(which, h).astype(BF16)
-        c = remote(bb.at[which, h], br.at[which, h], b_send.at[which, h], b_recv.at[which, h],
-                   {"sp": (2 * wrap(zh + h + 1, nh) + zl) * ny + y})
-        c.start()
-        b_copies[which, h] = c
-
-    def final_sum(which):
-        t = b_sum(which, nh - 1)
-        for h in range(nh - 1):
-            b_copies[which, h].wait()
-            t = t + br[which, h].astype(F32)
-        wgrad_ref[which] = t
-
-    for h in range(nh):
-        a_step(2, h)
-
+    weight_own_part(go, act, 2, 1, (nz - 2,))
+    edge_step(2, nz - 2)
+    middle_step(2, 0)
     step = 4
     for g in range(groups):
         def tap_block(b, accs, g=g):
@@ -457,37 +480,11 @@
         c.start()
         tzc.append(c)
 
-    weight_own_part(bi, sl, 0, 2)
-
-    for h in range(nh - 1):
-        b_step(2, h)
-
-    def first_part(which, h):
-        a_step(which, h)
-        if h < nh - 1:
-            b_step(which, h)
-
-    if nh > 1:
-        a_step(0, 0)
-    t = tg[...]
-    for o in range(1, nz):
-        tzc[o - 1].wait()
-        t = t + tgzr[o - 1]
-    tgz[...] = t
-    tyc = []
-    for r in range(1, ny):
-        c = remote(tgz, tgy.at[r - 1], ty_send.at[r - 1], ty_recv.at[r - 1], {"sp": z * ny + wrap(y + r, ny)})
-        c.start()
-        tyc.append(c)
-    for o in range(nz - 1 if nh > 1 else nz - 2, nz):
-        y_start(0, o)
-        y_start(1, o)
-    for h in range(nh - 1):
-        if h > 0:
-            a_step(0, h)
-        b_step(0, h)
-        a_step(1, h)
-        b_step(1, h)
+    weight_own_part(go, act, 2, 1, (nz - 1,))
+    for u in range(1, nz - 2):
+        middle_step(2, u)
+    weight_own_part(bi, sl, 0, 2, range(nz))
+    middle_step(2, nz - 2)
 
     def input_own(i):
         t = input_part(i, x)
@@ -496,11 +493,36 @@
             t = t + xr[o - 1, i].astype(F32)
         ig_ref[i * MATMUL_ROWS:(i + 1) * MATMUL_ROWS, :] = t.astype(BF16)
 
-    a_step(0, nh - 1)
-    a_step(1, nh - 1)
+    queue = []
+    for u in range(0, nz - 2, 2):
+        for which in range(2):
+            queue += [(which, v) for v in (u, u + 1) if v < nz - 2]
+    queue += [(0, nz - 2), (1, nz - 2)]
+    middle = queue[:-3] + [queue[-2], queue[-3], queue[-1]]
+    tyc = []
+    for n, item in enumerate(queue):
+        edge_step(*item)
+        if n == 3:
+            t = tg[...]
+            for o in range(1, nz):
+                tzc[o - 1].wait()
+                t = t + tgzr[o - 1]
+            tgz[...] = t
+            for r in range(1, ny):
+                c = remote(tgz, tgy.at[r - 1], ty_send.at[r - 1], ty_recv.at[r - 1],
+                           {"sp": z * ny + wrap(y + r, ny)})
+                c.start()
+                tyc.append(c)
+            y_start(0, nz - 1)
+            y_start(1, nz - 1)
+        if n > 0:
+            middle_step(*middle[n - 1])
+        if n < 2 * nrc and n % 2 == 0:
+            input_own(n // 2)
+    middle_step(*middle[-1])
+    for i in range(min(nrc, (len(queue) + 1) // 2), nrc):
+        input_own(i)
     final_sum(2)
-    for i in range(nrc):
-        input_own(i)
     t = tgz[...]
     for r in range(1, ny):
         tyc[r - 1].wait()
@@ -509,6 +531,9 @@
     gaingrad_ref[...] = t[tap_count:tap_count + 1]
     final_sum(0)
     final_sum(1)
+    for which in range(3):
+        for u in range(nz - 1):
+            chain_copy(which, u).wait_send()
 
     @pl.when(has_next)
     def _():
@@ -536,8 +561,6 @@
     nx = ntp // 2
     ny = nx
     nz = nsp // ny
-    nh = nz // 2
-    nb_slots = max(nh - 1, 1)
     groups = cl // LANES
     ds = width // nsp
     dt = width // ntp
@@ -571,8 +594,7 @@
             vm((2, 8, LANES), F32), vm((ntp - 1, 2, 8, LANES), F32),
             vm((rows, LANES), F32), vm((rows, LANES), F32),
             vm((3, nsp, ds, cl), BF16), vm((3, ny - 1, nz, ds, cl), BF16),
-            vm((3, nh, ds, cl), BF16), vm((3, nh, ds, cl), BF16),
-            vm((3, nb_slots, ds, cl), BF16), vm((3, nb_slots, ds, cl), BF16),
+            vm((3, nz - 1, ds, cl), BF16), vm((3, nz + 1, ds, cl), BF16),
             vm((nx - 1, nrc, MATMUL_ROWS, dt), BF16), vm((nx - 1, nrc, MATMUL_ROWS, dt), BF16),
             vm((tpad, cl), F32), vm((ny - 1, tpad, cl), F32),
             vm((tpad, cl), F32), vm((nz - 1, tpad, cl), F32),
@@ -582,8 +604,7 @@
             dma((nrc,)), dma((nrc,)),
             dma((nx - 1, nrc)), dma((nx - 1, nrc)),
             dma((3, ny - 1, nz)), dma((3, ny - 1, nz)),
-            dma((3, nh)), dma((3, nh)),
-            dma((3, nb_slots)), dma((3, nb_slots)),
+            dma((3, nz - 1)), dma((3, nz + 1)),
             dma((ny - 1,)), dma((ny - 1,)),
             dma((nz - 1,)), dma((nz - 1,)),
         ],

time: 61.7 us -> 56 us (0.908)
  Pallas kernels: 60.8 us -> 55 us
    pallas_call x1, Pallas kernels: 59.5 us -> 53.7 us  [shards(): pl.pallas_call(functools.partial(kernel, (nsp, ntp, ny, nz, nx, float(cha...]
where the time goes in v3:
time: 56 us; the launch traced here: 55.8 us
  Pallas kernels  55 us (98%)
  between operations  0.8 us (1%)
    pallas_call x1, Pallas kernels, shards(): pl.pallas_call(functools.partial(kernel, (nsp, ntp, ny, nz, nx, float(cha...  53.7 us
    pallas_call x1, Pallas kernels, shards(): pl.pallas_call(hand_out, out_shape=(jax.ShapeDtypeStruct((rows, dt), BF16...  1.29 us

profile of v3, /device:TPU:0, one launch (start us, length us, event | category | flops | bytes accessed | tf_op | source)
XLA Modules:
  0.0 55.8 jit_solution(6137471650889002938)
XLA Ops:
  0.6 53.7 %shard_map.118 = (bf16[1024,512]{1,0:T(8,128)(2,1)S(1)}, f32[3,256,256]{2,1,0:T(8,128)S(1)}, f32[31,256]{1,0:T(8,128)S(1)}, f32[1,256]{1,0:T(1,128)S(1)}) custom-call(bf16[1024,2048]{1,0:T(8,128)(2,1)} %bi_hbm.1, bf16[2048,256]{1,0:T(8,128)(2,1)} %wv_hbm.1, bf16[2048,256]{1,0:T(8,128)(2,1)} %wg_hbm.1, f32[31,256]{1,0:T(8,128)} %taps_hbm.1, ...), custom_call_target="tpu_custom_call" | custom-call | tf_op jit(solution)/shard_map/pallas_call | solution.py:576
  54.4 1.3 %shard_map.119 = (bf16[1024,512]{1,0:T(8,128)(2,1)}, f32[256,256]{1,0:T(8,128)}, f32[256,256]{1,0:T(8,128)}, f32[256,256]{1,0:T(8,128)}, f32[31,256]{1,0:T(8,128)}, /*index=5*/f32[1,256]{1,0:T(1,128)}) custom-call(bf16[1024,512]{1,0:T(8,128)(2,1)S(1)} %get-tuple-element.16.ig, f32[3,256,256]{2,1,0:T(8,128)S(1)} %get-tuple-element.17.wgrad, ...), custom_call_target="tpu_custom_call" | custom-call | tf_op jit(solution)/shard_map/pallas_call | solution.py:615

commit v4 on v3

--- a/solution.py
+++ b/solution.py
@@ -12,6 +12,7 @@
 ROW_BLOCK = 128
 MATMUL_ROWS = 256
 PAD = 32
+EARLY_FROM = 4
 F32 = jnp.float32
 BF16 = jnp.bfloat16
 MESH = pl.DeviceIdType.MESH
@@ -28,10 +29,10 @@
 def kernel(cfg, bi_hbm, wv_hbm, wg_hbm, taps_hbm, gain_hbm, wo_hbm, go_hbm,
            ig_ref, wgrad_ref, tgrad_ref, gaingrad_ref,
            bi, wv, wg, wo, go, taps_ref, gain_ref, val, sg, slope, hist, nrm, nsl, fut, act, sl, psl, pw,
-           st1, st1r, st2, st2r, spa, spb, gb, yb, zb, zin,
-           xs, xr, tg, tgy, tgz, tgzr,
+           st1, st1r, st2, st2r, spa, spb, gb, yb, zb, zin, eb, ein, ey, ef,
+           xs, xr, tg, tgb, tgy, tgz, tgzr,
            ld_sem, halo_sem, st_send, st_recv, pw_send, pw_recv, sl_send, sl_recv,
-           x_send, x_recv, y_send, y_recv, z_send, z_recv, ty_send, ty_recv, tz_send, tz_recv):
+           x_send, x_recv, y_send, y_recv, z_send, z_recv, e_send, e_recv, ey_send, ey_recv, ty_send, ty_recv, tz_send, tz_recv):
     nsp, ntp, ny, nz, nx, chan = cfg
     rows, width = bi.shape
     cl = wv.shape[1]
@@ -263,11 +264,14 @@
 
     peers = [(u, r) for u in range(nz) for r in range(1, ny)]
 
+    half = ds * EARLY_FROM // 8
+    share_rows = (ds, ds, half)
     y_copies = {}
     for which in range(3):
         for o, r in peers:
             yy = wrap(y + r, ny)
-            y_copies[which, o, r] = remote(gb.at[which, plane(o) * ny + yy], yb.at[which, r - 1, o],
+            rs = pl.ds(0, share_rows[which])
+            y_copies[which, o, r] = remote(gb.at[which, plane(o) * ny + yy, rs], yb.at[which, r - 1, o, rs],
                                            y_send.at[which, r - 1, o], y_recv.at[which, r - 1, o],
                                            {"sp": z * ny + yy})
 
@@ -275,83 +279,155 @@
         for r in range(1, ny):
             y_copies[which, o, r].start()
 
-    def weight_chunk(src, right, first, count, chunk):
+    def weight_chunk(src, right, first, count, chunk, between=None):
         cols = pl.ds(pl.multiple_of(chunk * per * ds, per * ds), per * ds)
-        t = dot_tn(src[:, cols], right[...]).astype(BF16)
+        if between is None:
+            t = dot_tn(src[:, cols], right[...])
+        else:
+            t = None
+            for k in range(nrc):
+                rs = pl.ds(k * MATMUL_ROWS, MATMUL_ROWS)
+                d = dot_tn(src[rs, cols], right[rs, :])
+                t = d if t is None else t + d
+                between(k)
+        t = t.astype(BF16)
         for j in range(per):
             for n in range(count):
                 gb[first + n, chunk * per + j] = t[j * ds:(j + 1) * ds, n * cl:(n + 1) * cl]
 
-    def weight_peer_part(src, right, first, count, started):
+    def weight_peer(src, right, first, count, o, between=None):
         if per == 1:
-            for o in range(nz):
-                for r in range(1, ny):
-                    weight_chunk(src, right, first, count, plane(o) * ny + wrap(y + r, ny))
-                started(o)
-        else:
+            for r in range(1, ny):
+                weight_chunk(src, right, first, count, plane(o) * ny + wrap(y + r, ny), between if r == 1 else None)
+            between = None
+        elif o == 0:
             for chunk in range(nsp // per):
                 weight_chunk(src, right, first, count, chunk)
-            for o in range(nz):
-                started(o)
-
-    def weight_own_part(src, right, first, count, planes):
+        if between is not None:
+            for k in range(nrc):
+                between(k)
+
+    def weight_own(src, right, first, count, o, between=None):
         if per == 1:
-            for o in planes:
-                weight_chunk(src, right, first, count, plane(o) * ny + y)
+            weight_chunk(src, right, first, count, plane(o) * ny + y, between)
+        elif between is not None:
+            for k in range(nrc):
+                between(k)
 
     def y_sum(which, u):
-        t = gb[which, plane(u) * ny + y].astype(F32)
+        n = share_rows[which]
+        t = gb[which, plane(u) * ny + y, 0:n].astype(F32)
         for r in range(1, ny):
             y_copies[which, u, r].wait()
-            t = t + yb[which, r - 1, u].astype(F32)
+            t = t + yb[which, r - 1, u, 0:n].astype(F32)
         return t
 
     def chain_in(which, slot):
-        return remote(zin.at[which, slot], zin.at[which, slot], z_send.at[which, 0], z_recv.at[which, slot],
+        rs = pl.ds(0, share_rows[which])
+        return remote(zin.at[which, slot, rs], zin.at[which, slot, rs], z_send.at[which, 0], z_recv.at[which, slot],
                       {"sp": wrap(z + 1, nz) * ny + y})
 
     edge = jnp.logical_or(z == 0, z == nz - 1)
 
+    def chain_to(u):
+        p = plane(u)
+        return jnp.where(p == z - 1, nz, p), {"sp": jnp.where(p > z, z + 1, z - 1) * ny + y}
+
     def chain_copy(which, u):
-        p = plane(u)
-        right = p > z
-        slot = jnp.where(p == z - 1, nz, p)
-        return remote(zb.at[which, u], zin.at[which, slot], z_send.at[which, u], z_recv.at[which, slot],
-                      {"sp": jnp.where(right, z + 1, z - 1) * ny + y})
+        slot, dev = chain_to(u)
+        rs = pl.ds(0, share_rows[which])
+        return remote(zb.at[which, u, rs], zin.at[which, slot, rs], z_send.at[which, u], z_recv.at[which, slot], dev)
 
     def edge_step(which, u):
         @pl.when(edge)
         def _():
-            zb[which, u] = y_sum(which, u).astype(BF16)
+            zb[which, u, 0:share_rows[which]] = y_sum(which, u).astype(BF16)
             chain_copy(which, u).start()
 
     def middle_step(which, u):
         @pl.when(jnp.logical_not(edge))
         def _():
+            n = share_rows[which]
             t = y_sum(which, u)
             chain_in(which, plane(u)).wait_recv()
-            zb[which, u] = (t + zin[which, plane(u)].astype(F32)).astype(BF16)
+            zb[which, u, 0:n] = (t + zin[which, plane(u), 0:n].astype(F32)).astype(BF16)
             chain_copy(which, u).start()
 
     def final_sum(which):
-        wgrad_ref[which] = y_sum(which, nz - 1)
+        n = share_rows[which]
+        wgrad_ref[which, 0:n] = y_sum(which, nz - 1)
 
         @pl.when(z > 0)
         def _():
             chain_in(which, z).wait_recv()
-            wgrad_ref[which] = wgrad_ref[which] + zin[which, z].astype(F32)
+            wgrad_ref[which, 0:n] = wgrad_ref[which, 0:n] + zin[which, z, 0:n].astype(F32)
 
         @pl.when(z < nz - 1)
         def _():
             chain_in(which, nz).wait_recv()
-            wgrad_ref[which] = wgrad_ref[which] + zin[which, nz].astype(F32)
-
-    def out_started(o):
-        if o == 0:
-            y_start(2, 0)
-
-    weight_peer_part(go, act, 2, 1, out_started)
-    weight_own_part(go, act, 2, 1, (0,))
+            wgrad_ref[which, 0:n] = wgrad_ref[which, 0:n] + zin[which, nz, 0:n].astype(F32)
+
+    def early_in(slot):
+        return remote(ein.at[slot], ein.at[slot], e_send.at[0], e_recv.at[slot], {"sp": wrap(z + 1, nz) * ny + y})
+
+    def early_copy(u, src):
+        slot, dev = chain_to(u)
+        return remote(src, ein.at[slot], e_send.at[u], e_recv.at[slot], dev)
+
+    def early_own(p):
+        return gb[2, pl.ds(p * ny, ny), half:ds].astype(F32)
+
+    def early_edge(u):
+        @pl.when(edge)
+        def _():
+            early_copy(u, gb.at[2, pl.ds(plane(u) * ny, ny), pl.ds(half, ds - half)]).start()
+
+    def early_middle(u):
+        @pl.when(jnp.logical_not(edge))
+        def _():
+            early_in(plane(u)).wait_recv()
+            eb[u] = (early_own(plane(u)) + ein[plane(u)].astype(F32)).astype(BF16)
+            early_copy(u, eb.at[u]).start()
+
+    early_y = []
+    for r in range(1, ny):
+        yy = wrap(y + r, ny)
+        early_y.append(remote(eb.at[nz - 1, yy], ey.at[r - 1], ey_send.at[r - 1], ey_recv.at[r - 1],
+                              {"sp": z * ny + yy}))
+
+    def early_turn():
+        ef[...] = early_own(z)
+
+        @pl.when(z > 0)
+        def _():
+            early_in(z).wait_recv()
+            ef[...] = ef[...] + ein[z].astype(F32)
+
+        @pl.when(z < nz - 1)
+        def _():
+            early_in(nz).wait_recv()
+            ef[...] = ef[...] + ein[nz].astype(F32)
+
+        eb[nz - 1] = ef[...].astype(BF16)
+        for c in early_y:
+            c.start()
+
+    def early_final():
+        t = ef[y]
+        for r in range(1, ny):
+            early_y[r - 1].wait()
+            t = t + ey[r - 1].astype(F32)
+        wgrad_ref[2, half:ds] = t
+
+    weight_peer(go, act, 2, 1, 0)
+    y_start(2, 0)
+    weight_own(go, act, 2, 1, 0)
+    early_edge(0)
+    weight_peer(go, act, 2, 1, 1)
+    y_start(2, 1)
+    weight_own(go, act, 2, 1, 1)
+    for o in range(2, nz - 1):
+        weight_peer(go, act, 2, 1, o)
 
     for c in st_copies:
         c.wait()
@@ -379,14 +455,15 @@
     def _():
         back.start()
 
-    for o in range(1, nz):
+    for o in range(2, nz - 1):
         y_start(2, o)
+    early_edge(1)
 
     lax.fori_loop(1, nb, slope_block, 0)
 
-    def adjoint_block(b, c):
+    def adjoint_block(b, only=None):
         r = pl.ds(pl.multiple_of(b * ROW_BLOCK, ROW_BLOCK), ROW_BLOCK)
-        for g in range(groups):
+        for g in range(groups) if only is None else only:
             acc = jnp.zeros((ROW_BLOCK, LANES), F32)
             for k in range(tap_count):
                 acc = acc + tap(k, g) * fut[g, pl.ds(b * ROW_BLOCK + k, ROW_BLOCK), :]
@@ -394,7 +471,6 @@
             t = acc * s
             sl[r, g * LANES:(g + 1) * LANES] = t.astype(BF16)
             sl[r, cl + g * LANES:cl + (g + 1) * LANES] = (t * val[g, r, :] * (1.0 - s)).astype(BF16)
-        return c
 
     def input_part(i, xx):
         r = slice(i * MATMUL_ROWS, (i + 1) * MATMUL_ROWS)
@@ -405,7 +481,6 @@
     xc = []
 
     def input_send(i):
-        slc[i].wait()
         for o in range(1, nx):
             xx = wrap(x + o, nx)
             xs[o - 1, i] = input_part(i, xx).astype(BF16)
@@ -418,46 +493,68 @@
         c.wait()
     slc = []
     for i in range(nrc):
+        if i == 2:
+            slc[0].wait()
+        todo = [(b, g) for b in range(i * bpc, nb - 1 if i == nrc - 1 else (i + 1) * bpc) for g in range(groups)]
+
+        def between(k, todo=todo):
+            for b, g in todo[k * len(todo) // nrc:(k + 1) * len(todo) // nrc]:
+                adjoint_block(b, (g,))
+
+        if not (i == 0 or i == 1):
+            for k in range(nrc):
+                between(k)
+        if i == 2:
+            input_send(0)
+        if i == 0:
+            for o in range(2, nz - 1):
+                weight_own(go, act, 2, 1, o, between if o == 2 else None)
+                early_edge(o)
+        if i == 1:
+            weight_peer(go, act, 2, 1, nz - 1, between)
+            y_start(2, nz - 1)
         if i == nrc - 1:
-            lax.fori_loop(i * bpc, nb - 1, adjoint_block, 0)
+            early_middle(0)
 
             @pl.when(has_next)
             def _():
                 back.wait_recv()
 
-            adjoint_block(nb - 1, 0)
-        else:
-            lax.fori_loop(i * bpc, (i + 1) * bpc, adjoint_block, 0)
+            adjoint_block(nb - 1)
         s = pl.ds(i * MATMUL_ROWS, MATMUL_ROWS)
         c = remote(sl.at[s], psl.at[s], sl_send.at[i], sl_recv.at[i], partner)
         c.start()
         slc.append(c)
-        if i > 0:
-            input_send(i - 1)
-        if i == 1:
-            edge_step(2, 0)
-        if i == 2:
-            weight_own_part(go, act, 2, 1, range(1, nz - 2))
-
-    def vg_started(o):
-        if o == nz - 2:
-            y_start(0, o)
-            y_start(1, o)
+
+    for o in range(nz):
+        weight_peer(bi, sl, 0, 2, o)
+        if o == 0:
+            y_start(0, 0)
         elif o < nz - 2 and (o % 2 == 1 or o == nz - 3):
             for which in range(2):
                 for v in range(o - o % 2, o + 1):
-                    y_start(which, v)
-
-    for u in range(1, nz - 2):
+                    if which or v:
+                        y_start(which, v)
+        elif o == nz - 2:
+            y_start(0, o)
+            y_start(1, o)
+
+    for u in range(nz - 1):
         edge_step(2, u)
-    weight_peer_part(bi, sl, 0, 2, vg_started)
+    for i in range(1, nrc - 1):
+        slc[i].wait()
+        input_send(i)
+    early_middle(1)
+    weight_own(go, act, 2, 1, nz - 1)
+    for o in range(nz):
+        weight_own(bi, sl, 0, 2, o)
+    edge_step(0, 0)
+    slc[nrc - 1].wait()
     input_send(nrc - 1)
-    weight_own_part(go, act, 2, 1, (nz - 2,))
-    edge_step(2, nz - 2)
-    middle_step(2, 0)
+
     step = 4
-    for g in range(groups):
-        def tap_block(b, accs, g=g):
+    def taps_part(g):
+        def tap_block(b, accs):
             r = b * 8 * step
             f = fut[g, pl.ds(pl.multiple_of(r, 8 * step), 8 * step), :]
             out = []
@@ -474,18 +571,6 @@
             tg[k:k + 1, g * LANES:(g + 1) * LANES] = jnp.sum(accs[k], axis=0, keepdims=True)
         tg[tap_count:tap_count + 1, g * LANES:(g + 1) * LANES] = jnp.sum(gacc[g], axis=0, keepdims=True)
 
-    tzc = []
-    for o in range(1, nz):
-        c = remote(tg, tgzr.at[o - 1], tz_send.at[o - 1], tz_recv.at[o - 1], {"sp": wrap(z + o, nz) * ny + y})
-        c.start()
-        tzc.append(c)
-
-    weight_own_part(go, act, 2, 1, (nz - 1,))
-    for u in range(1, nz - 2):
-        middle_step(2, u)
-    weight_own_part(bi, sl, 0, 2, range(nz))
-    middle_step(2, nz - 2)
-
     def input_own(i):
         t = input_part(i, x)
         for o in range(1, nx):
@@ -499,40 +584,68 @@
             queue += [(which, v) for v in (u, u + 1) if v < nz - 2]
     queue += [(0, nz - 2), (1, nz - 2)]
     middle = queue[:-3] + [queue[-2], queue[-3], queue[-1]]
+
+    taps_part(0)
+    for u in range(2, nz - 1):
+        early_middle(u)
+    middle_step(2, 0)
+    edge_step(*queue[1])
+    for g in range(1, groups):
+        taps_part(g)
+    tgb[...] = tg[...].astype(BF16)
+    tzc = []
+    for o in range(1, nz):
+        c = remote(tgb, tgzr.at[o - 1], tz_send.at[o - 1], tz_recv.at[o - 1], {"sp": wrap(z + o, nz) * ny + y})
+        c.start()
+        tzc.append(c)
+
+    for u in range(1, nz - 2):
+        middle_step(2, u)
+    edge_step(*queue[2])
+    middle_step(2, nz - 2)
+    middle_step(*middle[0])
+    early_turn()
+    y_start(0, nz - 1)
+    edge_step(*queue[3])
     tyc = []
-    for n, item in enumerate(queue):
-        edge_step(*item)
-        if n == 3:
-            t = tg[...]
+    done = 0
+    for n in range(1, len(queue)):
+        middle_step(*middle[n])
+        if n == 1:
+            input_own(done)
+            done += 1
+        if n + 3 < len(queue):
+            edge_step(*queue[n + 3])
+        if n == 2:
+            t = tgb[...].astype(F32)
             for o in range(1, nz):
                 tzc[o - 1].wait()
-                t = t + tgzr[o - 1]
-            tgz[...] = t
+                t = t + tgzr[o - 1].astype(F32)
+            tgz[...] = t.astype(BF16)
             for r in range(1, ny):
                 c = remote(tgz, tgy.at[r - 1], ty_send.at[r - 1], ty_recv.at[r - 1],
                            {"sp": z * ny + wrap(y + r, ny)})
                 c.start()
                 tyc.append(c)
-            y_start(0, nz - 1)
             y_start(1, nz - 1)
-        if n > 0:
-            middle_step(*middle[n - 1])
-        if n < 2 * nrc and n % 2 == 0:
-            input_own(n // 2)
-    middle_step(*middle[-1])
-    for i in range(min(nrc, (len(queue) + 1) // 2), nrc):
+        if n > 2 and done < nrc - 1:
+            input_own(done)
+            done += 1
+    for i in range(done, nrc):
         input_own(i)
+    early_final()
     final_sum(2)
-    t = tgz[...]
+    t = tgz[...].astype(F32)
     for r in range(1, ny):
         tyc[r - 1].wait()
-        t = t + tgy[r - 1]
+        t = t + tgy[r - 1].astype(F32)
     tgrad_ref[...] = t[0:tap_count]
     gaingrad_ref[...] = t[tap_count:tap_count + 1]
     final_sum(0)
     final_sum(1)
-    for which in range(3):
-        for u in range(nz - 1):
+    for u in range(nz - 1):
+        early_copy(u, eb.at[u]).wait_send()
+        for which in range(3):
             chain_copy(which, u).wait_send()
 
     @pl.when(has_next)
@@ -563,6 +676,7 @@
     nz = nsp // ny
     groups = cl // LANES
     ds = width // nsp
+    late = ds - ds * EARLY_FROM // 8
     dt = width // ntp
     nrc = rows // MATMUL_ROWS
     tap_count = conv_taps.shape[0]
@@ -570,7 +684,7 @@
     vm = pltpu.VMEM
     wide = vm((groups, rows, LANES), F32)
     padded = vm((groups, rows + PAD, LANES), F32)
-    tpad = -(-(tap_count + 1) // 8) * 8
+    tpad = -(-(tap_count + 1) // 16) * 16
     any_spec = pl.BlockSpec(memory_space=pltpu.HBM)
     vmem_spec = pl.BlockSpec(memory_space=pltpu.VMEM)
     outs = pl.pallas_call(
@@ -595,9 +709,11 @@
             vm((rows, LANES), F32), vm((rows, LANES), F32),
             vm((3, nsp, ds, cl), BF16), vm((3, ny - 1, nz, ds, cl), BF16),
             vm((3, nz - 1, ds, cl), BF16), vm((3, nz + 1, ds, cl), BF16),
+            vm((nz, ny, late, cl), BF16), vm((nz + 1, ny, late, cl), BF16),
+            vm((ny - 1, late, cl), BF16), vm((ny, late, cl), F32),
             vm((nx - 1, nrc, MATMUL_ROWS, dt), BF16), vm((nx - 1, nrc, MATMUL_ROWS, dt), BF16),
-            vm((tpad, cl), F32), vm((ny - 1, tpad, cl), F32),
-            vm((tpad, cl), F32), vm((nz - 1, tpad, cl), F32),
+            vm((tpad, cl), F32), vm((tpad, cl), BF16), vm((ny - 1, tpad, cl), BF16),
+            vm((tpad, cl), BF16), vm((nz - 1, tpad, cl), BF16),
             dma((6 + nrc,)), dma((4,)),
             dma((2, ntp - 1)), dma((2, ntp - 1)),
             dma((nx, 2)), dma((nx, 2)),
@@ -605,6 +721,7 @@
             dma((nx - 1, nrc)), dma((nx - 1, nrc)),
             dma((3, ny - 1, nz)), dma((3, ny - 1, nz)),
             dma((3, nz - 1)), dma((3, nz + 1)),
+            dma((nz - 1,)), dma((nz + 1,)), dma((ny - 1,)), dma((ny - 1,)),
             dma((ny - 1,)), dma((ny - 1,)),
             dma((nz - 1,)), dma((nz - 1,)),
         ],

time: 56 us -> 53.4 us (0.954)
  Pallas kernels: 55 us -> 52.4 us
    pallas_call x1, Pallas kernels: 53.7 us -> 51.1 us  [shards(): pl.pallas_call(functools.partial(kernel, (nsp, ntp, ny, nz, nx, float(cha...]
where the time goes in v4:
time: 53.4 us; the launch traced here: 53.2 us
  Pallas kernels  52.4 us (98%)
  between operations  0.8 us (1%)
    pallas_call x1, Pallas kernels, shards(): pl.pallas_call(functools.partial(kernel, (nsp, ntp, ny, nz, nx, float(cha...  51.1 us
    pallas_call x1, Pallas kernels, shards(): pl.pallas_call(hand_out, out_shape=(jax.ShapeDtypeStruct((rows, dt), BF16...  1.29 us

profile of v4, /device:TPU:0, one launch (start us, length us, event | category | flops | bytes accessed | tf_op | source)
XLA Modules:
  0.0 53.2 jit_solution(12481850361945917748)
XLA Ops:
  0.6 51.1 %shard_map.118 = (bf16[1024,512]{1,0:T(8,128)(2,1)S(1)}, f32[3,256,256]{2,1,0:T(8,128)S(1)}, f32[31,256]{1,0:T(8,128)S(1)}, f32[1,256]{1,0:T(1,128)S(1)}) custom-call(bf16[1024,2048]{1,0:T(8,128)(2,1)} %bi_hbm.1, bf16[2048,256]{1,0:T(8,128)(2,1)} %wv_hbm.1, bf16[2048,256]{1,0:T(8,128)(2,1)} %wg_hbm.1, f32[31,256]{1,0:T(8,128)} %taps_hbm.1, ...), custom_call_target="tpu_custom_call" | custom-call | tf_op jit(solution)/shard_map/pallas_call | solution.py:690
  51.8 1.3 %shard_map.119 = (bf16[1024,512]{1,0:T(8,128)(2,1)}, f32[256,256]{1,0:T(8,128)}, f32[256,256]{1,0:T(8,128)}, f32[256,256]{1,0:T(8,128)}, f32[31,256]{1,0:T(8,128)}, /*index=5*/f32[1,256]{1,0:T(1,128)}) custom-call(bf16[1024,512]{1,0:T(8,128)(2,1)S(1)} %get-tuple-element.16.ig, f32[3,256,256]{2,1,0:T(8,128)S(1)} %get-tuple-element.17.wgrad, ...), custom_call_target="tpu_custom_call" | custom-call | tf_op jit(solution)/shard_map/pallas_call | solution.py:732

commit v5 on v4

--- a/solution.py
+++ b/solution.py
@@ -163,6 +163,7 @@
             loads["gain"].wait()
             for j in reversed(range(nrc - 1)):
                 loads["bi%d" % j].wait()
+        if n == 1:
             pl.semaphore_wait(barrier, nsp + ntp - 2)
 
             @pl.when(has_next)
@@ -528,14 +529,7 @@
 
     for o in range(nz):
         weight_peer(bi, sl, 0, 2, o)
-        if o == 0:
-            y_start(0, 0)
-        elif o < nz - 2 and (o % 2 == 1 or o == nz - 3):
-            for which in range(2):
-                for v in range(o - o % 2, o + 1):
-                    if which or v:
-                        y_start(which, v)
-        elif o == nz - 2:
+        if o < nz - 1:
             y_start(0, o)
             y_start(1, o)
 
@@ -578,12 +572,8 @@
             t = t + xr[o - 1, i].astype(F32)
         ig_ref[i * MATMUL_ROWS:(i + 1) * MATMUL_ROWS, :] = t.astype(BF16)
 
-    queue = []
-    for u in range(0, nz - 2, 2):
-        for which in range(2):
-            queue += [(which, v) for v in (u, u + 1) if v < nz - 2]
-    queue += [(0, nz - 2), (1, nz - 2)]
-    middle = queue[:-3] + [queue[-2], queue[-3], queue[-1]]
+    queue = [(which, u) for u in range(nz - 1) for which in range(2)]
+    middle = queue[:-4] + [queue[-2], queue[-4], queue[-1], queue[-3]]
 
     taps_part(0)
     for u in range(2, nz - 1):

time: 53.4 us -> 51.3 us (0.961)
  Pallas kernels: 52.4 us -> 50.4 us
    pallas_call x1, Pallas kernels: 51.1 us -> 49.1 us  [shards(): pl.pallas_call(functools.partial(kernel, (nsp, ntp, ny, nz, nx, float(cha...]
where the time goes in v5:
time: 51.3 us; the launch traced here: 51.2 us
  Pallas kernels  50.4 us (98%)
  between operations  0.8 us (2%)
    pallas_call x1, Pallas kernels, shards(): pl.pallas_call(functools.partial(kernel, (nsp, ntp, ny, nz, nx, float(cha...  49.1 us
    pallas_call x1, Pallas kernels, shards(): pl.pallas_call(hand_out, out_shape=(jax.ShapeDtypeStruct((rows, dt), BF16...  1.29 us

profile of v5, /device:TPU:0, one launch (start us, length us, event | category | flops | bytes accessed | tf_op | source)
XLA Modules:
  0.0 51.2 jit_solution(14013735311297806875)
XLA Ops:
  0.6 49.1 %shard_map.118 = (bf16[1024,512]{1,0:T(8,128)(2,1)S(1)}, f32[3,256,256]{2,1,0:T(8,128)S(1)}, f32[31,256]{1,0:T(8,128)S(1)}, f32[1,256]{1,0:T(1,128)S(1)}) custom-call(bf16[1024,2048]{1,0:T(8,128)(2,1)} %bi_hbm.1, bf16[2048,256]{1,0:T(8,128)(2,1)} %wv_hbm.1, bf16[2048,256]{1,0:T(8,128)(2,1)} %wg_hbm.1, f32[31,256]{1,0:T(8,128)} %taps_hbm.1, ...), custom_call_target="tpu_custom_call" | custom-call | tf_op jit(solution)/shard_map/pallas_call | solution.py:680
  49.7 1.3 %shard_map.119 = (bf16[1024,512]{1,0:T(8,128)(2,1)}, f32[256,256]{1,0:T(8,128)}, f32[256,256]{1,0:T(8,128)}, f32[256,256]{1,0:T(8,128)}, f32[31,256]{1,0:T(8,128)}, /*index=5*/f32[1,256]{1,0:T(1,128)}) custom-call(bf16[1024,512]{1,0:T(8,128)(2,1)S(1)} %get-tuple-element.16.ig, f32[3,256,256]{2,1,0:T(8,128)S(1)} %get-tuple-element.17.wgrad, ...), custom_call_target="tpu_custom_call" | custom-call | tf_op jit(solution)/shard_map/pallas_call | solution.py:722
